TPU v7x, 32 devices: a whole 2x2x4 slice. The times are simulated.
32 devices in a mesh: sp: 8 (over z, x), tp: 4 (over y, core).
Axes of the slice: x: 2, y: 2, z: 4, core: 2. Of those that a mesh axis runs over, the one named last changes fastest.
Arguments:
- stream: bfloat16 [1024, 2048], P('sp', 'tp')
- norm_gain: float32 [2048], P('tp'), may hold values from 0.1 to 1.9
- w_value: bfloat16 [2048, 512], P(None, 'tp'), may hold values from -0.125 to 0.125
- w_mix: bfloat16 [2048, 512], P(None, 'tp'), may hold values from -0.125 to 0.125
- w_gate: bfloat16 [2048, 512], P(None, 'tp'), may hold values from -0.125 to 0.125
- w_state: bfloat16 [2048, 512], P(None, 'tp'), may hold values from -0.125 to 0.125
- conv_taps: float32 [3, 512], P(None, 'tp'), may hold values from -3 to 3
- skip_gain: float32 [512], P('tp'), may hold values from -3 to 3
- decay_rate: float32 [2, 32, 64], P(None, 'tp'), as said below
- turn_rate: float32 [2, 32, 64], P(None, 'tp'), may hold values from 0.25 to 1.5
- input_real: float32 [2, 32, 64, 16], P(None, 'tp')
- input_imag: float32 [2, 32, 64, 16], P(None, 'tp')
- read_real: float32 [2, 32, 16, 64], P(None, 'tp'), may hold values from -0.75 to 0.75
- read_imag: float32 [2, 32, 16, 64], P(None, 'tp'), may hold values from -0.75 to 0.75
- initial_state: float32 [2, 2, 32, 64], P(None, None, 'tp'), may hold values from -5 to 5
- intervals: float32 [1024], P('sp'), as said below
- proj_conv: bfloat16 [512, 2048], P('tp'), may hold values from -0.1875 to 0.1875
- proj_state: bfloat16 [512, 2048], P('tp'), may hold values from -0.1875 to 0.1875
Outputs:
- mixed: bfloat16 [1024, 2048], P('sp', 'tp')
Inputs may be any that keep to these rules, and one draw needn't show every extreme that they name: `decay_rate`: Positive. `intervals`: Positive.
All inputs are finite; a program needn't handle non-finite values.
Results may differ from a plain program's by a relative error of at most 0.024.
Values may be sent and summed in bfloat16 or wider, within the bound.
A program may use at most 64 MiB of HBM per device.

v0:
```python
import functools

import jax
import jax.numpy as jnp
from jax import lax
from jax.experimental import pallas as pl
from jax.experimental.pallas import tpu as pltpu
from jax.sharding import PartitionSpec as P

EPSILON = 1e-06
MESH = pl.DeviceIdType.MESH
F32 = jnp.float32
BF16 = jnp.bfloat16
CHUNKS = 2
OUT_CHUNKS = 2


def dot(a, b):
    return jnp.dot(a, b, preferred_element_type=F32)


def dot_t(a, b):
    return lax.dot_general(a, b, (((1,), (1,)), ((), ())), preferred_element_type=F32)


def half_turns(angle):
    theta = 0.5 * angle
    n = jnp.floor(theta * 0.6366197723675814 + 0.5)
    r = theta - n * 1.5703125
    r = r - n * 0.00048351287841796875
    r = r - n * 3.1385570764541626e-07
    r = r - n * 6.077100627776710e-11
    odd = (n - 2.0 * jnp.floor(0.5 * n)) > 0.5
    z = r * r
    s = r + r * z * ((-1.9515295891e-4 * z + 8.3321608736e-3) * z - 1.6666654611e-1)
    c = 1.0 - 0.5 * z + z * z * (
        (2.443315711809948e-5 * z - 1.388731625493765e-3) * z + 4.166664568298827e-2
    )
    square = jnp.where(odd, c * c, s * s)
    double = 2.0 * s * c
    return square, jnp.where(odd, -double, double)


def expm1_of(x, e):
    p = 1.0 + x * (1.0 / 7.0)
    for k in (6.0, 5.0, 4.0, 3.0, 2.0):
        p = 1.0 + x * p * (1.0 / k)
    return jnp.where(x > -0.35, x * p, e - 1.0)


def repeat(lo, hi, body):
    if hi - lo <= 16:
        for i in range(lo, hi):
            body(i)
    else:
        def step(i, carry):
            body(i)
            return carry
        lax.fori_loop(lo, hi, step, 0)


def kernel(
    n_sp, n_tp,
    x_hbm, gain_hbm, wv, wm, wg, ws, taps_hbm, skip_hbm, decay_hbm, turn_hbm,
    inr, ini, rdr, rdi, init_hbm, iv_hbm, pc, ps,
    out_ref,
    x_ref, gain_ref, taps_ref, skip_ref, decay_ref, turn_ref, init_ref, iv_s,
    w_all, p_all, in_v, rd_v, x_full, gains, el_all, fr_ref, fi_ref, gr_ref, gi_ref,
    dr_ref, di_ref, h0r, h0i, h1r, h1i, bt_ref, rt_ref, src_ref, halo_ref, e_out, e_all,
    blk_r, blk_i, p1_out, p1_in, p2_out, p2_in, c_out, c_in,
    load_sem, as_sem, ar_sem, bs_sem, br_sem, fs_sem, fwr_sem, gs_sem, grv_sem,
    is_sem, ir_sem, hs_sem, hr_sem, es_sem, er_sem, p1s, p1r, p2s, p2r, cs, cr,
):
    tp, sp = lax.axis_index("tp"), lax.axis_index("sp")
    rows, width = x_hbm.shape
    channels = wv.shape[1]
    y, core = tp // 2, tp % 2
    sib = y * 2 + 1 - core
    oth = (1 - y) * 2 + core
    diag = (1 - y) * 2 + 1 - core
    cw = width // CHUNKS

    loads = []

    def load(src, dst):
        copy = pltpu.make_async_copy(src, dst, load_sem.at[len(loads)])
        copy.start()
        loads.append(copy)

    barrier = pltpu.get_barrier_semaphore()
    for j in range(1, n_tp):
        pl.semaphore_signal(barrier, inc=1, device_id={"tp": (tp + j) % n_tp}, device_id_type=MESH)
    repeat(1, n_sp, lambda r: pl.semaphore_signal(
        barrier, inc=1, device_id={"sp": (sp + r) % n_sp}, device_id_type=MESH))
    load(iv_hbm, iv_s)
    load(decay_hbm, decay_ref)
    load(turn_hbm, turn_ref)
    load(init_hbm, init_ref)
    load(inr, in_v.at[0])
    load(ini, in_v.at[1])
    load(rdr, rd_v.at[0])
    load(rdi, rd_v.at[1])
    load(x_hbm, x_ref)
    load(gain_hbm, gain_ref)
    for j, w in enumerate((wv, wm, wg, ws)):
        load(w, w_all.at[:, pl.ds(j * channels, channels)])
    load(taps_hbm, taps_ref)
    load(skip_hbm, skip_ref)
    load(pc, p_all.at[pl.ds(0, channels)])
    load(ps, p_all.at[pl.ds(channels, channels)])
    pl.semaphore_wait(barrier, n_tp - 1 + n_sp - 1)

    def remote(src, dst, send, recv, where):
        return pltpu.make_async_remote_copy(
            src_ref=src, dst_ref=dst, send_sem=send, recv_sem=recv,
            device_id=where, device_id_type=MESH)

    to_sib, to_oth, forward = [], [], []
    for c in range(CHUNKS):
        piece = x_hbm.at[:, pl.ds(c * cw, cw)]
        to_oth.append(remote(piece, x_full.at[tp, c], bs_sem.at[c], br_sem.at[c], {"tp": oth}))
        to_sib.append(remote(piece, x_full.at[tp, c], as_sem.at[c], ar_sem.at[c], {"tp": sib}))
        forward.append(remote(x_full.at[oth, c], x_full.at[oth, c], fs_sem.at[c], fwr_sem.at[c],
                              {"tp": sib}))
    gain_copies = [
        remote(gain_hbm, gains.at[tp], gs_sem.at[j], grv_sem.at[j], {"tp": (tp + j) % n_tp})
        for j in range(1, n_tp)
    ]
    for copy in gain_copies:
        copy.start()
    for c in range(CHUNKS):
        to_oth[c].start()
        to_sib[c].start()

    def interval_copy(r):
        return remote(iv_hbm, el_all.at[r], is_sem.at[r], ir_sem.at[r], {"sp": (sp + r) % n_sp})

    repeat(1, n_sp, lambda r: interval_copy(r).start())

    sub = lax.broadcasted_iota(jnp.int32, (8, 128), 0)
    top = sub < 4

    def pack(ref):
        even = ref[pl.ds(0, 8, stride=2), :]
        odd = ref[pl.ds(1, 8, stride=2), :]
        return jnp.concatenate([even, odd], axis=1)

    for i in range(4):
        loads[i].wait()
    decay, turn = pack(decay_ref), pack(turn_ref)

    def pack_init(part):
        halves = [
            jnp.concatenate([init_ref[pl.ds(d * 16 + part * 8, 4, stride=2), :],
                             init_ref[pl.ds(d * 16 + part * 8 + 1, 4, stride=2), :]], axis=1)
            for d in range(2)
        ]
        return jnp.concatenate(halves, axis=0)

    init_r, init_i = pack_init(0), pack_init(1)
    den = decay * decay + turn * turn
    td, dd = turn / den, decay / den

    def factors(k, carry):
        iv = jnp.where(top, iv_s[0, k], iv_s[0, rows - 1 - k])
        damp = -decay * iv
        square, sine = half_turns(turn * iv)
        e = jnp.exp(damp)
        cosine = 1.0 - 2.0 * square
        f_im = e * sine
        lift = expm1_of(damp, e) * cosine - 2.0 * square
        at = pl.ds(pl.multiple_of(k * 8, 8), 8)
        fr_ref[at, :] = e * cosine
        fi_ref[at, :] = f_im
        gr_ref[at, :] = td * f_im - dd * lift
        gi_ref[at, :] = -(dd * f_im + td * lift)
        return carry

    for c in range(CHUNKS):
        lax.fori_loop(c * rows // CHUNKS, (c + 1) * rows // CHUNKS, factors, 0, unroll=4)
        to_oth[c].wait_recv()
        forward[c].start()

    for i in range(4, 8):
        loads[i].wait()
    states = bt_ref.shape[2]
    per = rd_v.shape[2]
    half = states // 2
    group = channels * per // half
    spread = (lax.broadcasted_iota(jnp.int32, (per, half), 1) % per
              == lax.broadcasted_iota(jnp.int32, (per, half), 0)).astype(BF16)
    keep = ((lax.broadcasted_iota(jnp.int32, (channels, half), 1) // per)
            == (lax.broadcasted_iota(jnp.int32, (channels, half), 0) // group))
    for part in range(2):
        for d in range(2):
            at, to = pl.ds(d * channels, channels), pl.ds(d * half, half)
            wide = dot(in_v[part, at, :].astype(BF16), spread)
            bt_ref[part, :, to] = jnp.where(keep, wide, 0.0).astype(BF16)
            wide = dot(rd_v[part, at, :].astype(BF16), spread)
            if part:
                wide = -wide
            rt_ref[part, :, to] = jnp.where(keep, wide, 0.0).astype(BF16)

    for i in range(8, 14):
        loads[i].wait()
    for copy in gain_copies:
        copy.wait_recv()

    def project(value, gain, first):
        wide = value.astype(F32)
        scaled = (wide * gain).astype(BF16)
        term = dot(scaled, w_all[pl.ds(pl.multiple_of(first, cw), cw), :])
        return term, jnp.sum(wide * wide, axis=1, keepdims=True)

    projected = jnp.zeros((rows, 4 * channels), F32)
    squares = jnp.zeros((rows, 1), F32)
    for c in range(CHUNKS):
        t, s = project(x_ref[:, c * cw:(c + 1) * cw], gain_ref[:, c * cw:(c + 1) * cw],
                       tp * width + c * cw)
        projected, squares = projected + t, squares + s

    def remaining(owner, waits, projected, squares):
        for c in range(CHUNKS):
            if waits is not None:
                waits[c].wait_recv()
            t, s = project(x_full[owner, c], gains[owner][:, c * cw:(c + 1) * cw],
                           owner * width + c * cw)
            projected, squares = projected + t, squares + s
        return projected, squares

    projected, squares = remaining(sib, to_sib, projected, squares)
    projected, squares = remaining(oth, None, projected, squares)
    projected, squares = remaining(diag, forward, projected, squares)
    projected = projected * lax.rsqrt(squares / (width * n_tp) + EPSILON)
    conv_value = projected[:, :channels].astype(BF16).astype(F32)
    conv_mix = projected[:, channels:2 * channels].astype(BF16).astype(F32)
    conv_gate = projected[:, 2 * channels:3 * channels].astype(BF16).astype(F32)
    state_input = projected[:, 3 * channels:].astype(BF16)
    src_ref[...] = (conv_mix * conv_value).astype(BF16)

    for part, ref in ((0, dr_ref), (1, di_ref)):
        driven = dot(state_input, bt_ref[part])
        for j in range(8):
            ref[pl.ds(j, rows, stride=8), :] = driven[:, j * 128:(j + 1) * 128]

    halo_up = remote(src_ref.at[pl.ds(rows - 16, 16)], halo_ref.at[0], hs_sem.at[0], hr_sem.at[0],
                     {"sp": (sp + 1) % n_sp})
    halo_down = remote(src_ref.at[pl.ds(0, 16)], halo_ref.at[1], hs_sem.at[1], hr_sem.at[1],
                       {"sp": (sp + n_sp - 1) % n_sp})
    halo_up.start()
    halo_down.start()

    def first_pass(k, carry):
        hr, hi = carry
        at = pl.ds(pl.multiple_of(k * 8, 8), 8)
        back = pl.ds(pl.multiple_of((rows - 1 - k) * 8, 8), 8)
        dr = jnp.where(top, dr_ref[at, :], dr_ref[back, :])
        di = jnp.where(top, di_ref[at, :], di_ref[back, :])
        gr, gi = gr_ref[at, :], gi_ref[at, :]
        fr, fi = fr_ref[at, :], fi_ref[at, :]
        pr = gr * dr - gi * di
        pi = gr * di + gi * dr
        gr_ref[at, :] = pr
        gi_ref[at, :] = pi
        return fr * hr + (pr - fi * hi), fr * hi + (pi + fi * hr)

    zero = jnp.zeros((8, 128), F32)
    hr, hi = lax.fori_loop(0, rows, first_pass, (zero, zero), unroll=8)
    e_out[0] = hr
    e_out[1] = hi

    def edge_copy(r):
        return remote(e_out, e_all.at[r], es_sem.at[r], er_sem.at[r], {"sp": (sp + r) % n_sp})

    repeat(1, n_sp, lambda r: edge_copy(r).start())

    repeat(1, n_sp, lambda r: interval_copy(r).wait_recv())

    def block_factor(r):
        before = jnp.sum(el_all[r], axis=1, keepdims=True) * jnp.where(sp - r >= 0, 1.0, 0.0)
        after = jnp.sum(el_all[n_sp - r], axis=1, keepdims=True) * jnp.where(sp + r < n_sp, 1.0, 0.0)
        elapsed = jnp.where(top, before, after)
        square, sine = half_turns(turn * elapsed)
        e = jnp.exp(-decay * elapsed)
        blk_r[r] = e * (1.0 - 2.0 * square)
        blk_i[r] = e * sine

    repeat(1, n_sp, block_factor)

    halo_up.wait_recv()
    halo_down.wait_recv()
    for i in range(14, 18):
        loads[i].wait()
    source = src_ref[...].astype(F32)
    line = lax.broadcasted_iota(jnp.int32, (rows, channels), 0)
    before = halo_ref[0].astype(F32)[15:16, :] * jnp.where(sp > 0, 1.0, 0.0)
    after = halo_ref[1].astype(F32)[0:1, :] * jnp.where(sp < n_sp - 1, 1.0, 0.0)
    previous = jnp.where(line == 0, before, pltpu.roll(source, 1, 0))
    following = jnp.where(line == rows - 1, after, pltpu.roll(source, rows - 1, 0))
    filtered = taps_ref[0:1, :] * previous + taps_ref[1:2, :] * source + taps_ref[2:3, :] * following
    conv_out = (conv_gate * filtered).astype(BF16)

    repeat(1, n_sp, lambda r: edge_copy(r).wait_recv())

    def combine(r, hr, hi):
        er = jnp.where(top, jnp.where(sp - r >= 0, e_all[r, 0], 0.0),
                       jnp.where(sp + r < n_sp, e_all[n_sp - r, 0], 0.0))
        ei = jnp.where(top, jnp.where(sp - r >= 0, e_all[r, 1], 0.0),
                       jnp.where(sp + r < n_sp, e_all[n_sp - r, 1], 0.0))
        fr, fi = blk_r[r], blk_i[r]
        return fr * hr + (er - fi * hi), fr * hi + (ei + fi * hr)

    hr, hi = init_r, init_i
    if n_sp <= 16:
        for r in range(n_sp - 1, 0, -1):
            hr, hi = combine(r, hr, hi)
    else:
        hr, hi = lax.fori_loop(1, n_sp, lambda i, h: combine(n_sp - i, *h), (hr, hi))

    def second_pass(k, carry):
        hr, hi = carry
        at = pl.ds(pl.multiple_of(k * 8, 8), 8)
        back = pl.ds(pl.multiple_of((rows - 1 - k) * 8, 8), 8)
        fr, fi = fr_ref[at, :], fi_ref[at, :]
        nr = fr * hr + (gr_ref[at, :] - fi * hi)
        ni = fr * hi + (gi_ref[at, :] + fi * hr)
        h0r[at, :] = nr
        h0i[at, :] = ni
        h1r[back, :] = nr
        h1i[back, :] = ni
        return nr, ni

    lax.fori_loop(0, rows, second_pass, (hr, hi), unroll=8)

    response = state_input.astype(F32) * skip_ref[...]
    for part, (forth, back) in enumerate(((h0r, h1r), (h0i, h1i))):
        history = jnp.concatenate(
            [(forth if j < 4 else back)[pl.ds(j, rows, stride=8), :].astype(BF16) for j in range(8)],
            axis=1)
        response = response + dot_t(history, rt_ref[part])
    inner = 0.7978845608028654 * (response + 0.044715 * (response * response * response))
    state_out = (0.5 * response * (1.0 + jnp.tanh(inner))).astype(BF16)
    branches = jnp.concatenate([conv_out, state_out], axis=1)

    ow = width // OUT_CHUNKS

    def partial(owner, c):
        return dot(branches, p_all[:, pl.ds(pl.multiple_of(owner * width + c * ow, ow), ow)])

    first, second, cross = [], [], []
    for c in range(OUT_CHUNKS):
        p1_out[c] = partial(diag, c).astype(BF16)
        first.append(remote(p1_out.at[c], p1_in.at[c], p1s.at[c], p1r.at[c], {"tp": sib}))
        first[c].start()
    kept = [partial(oth, c) for c in range(OUT_CHUNKS)]
    for c in range(OUT_CHUNKS):
        first[c].wait_recv()
        c_out[c] = (kept[c] + p1_in[c].astype(F32)).astype(BF16)
        cross.append(remote(c_out.at[c], c_in.at[c], cs.at[c], cr.at[c], {"tp": oth}))
        cross[c].start()
    for c in range(OUT_CHUNKS):
        p2_out[c] = partial(sib, c).astype(BF16)
        second.append(remote(p2_out.at[c], p2_in.at[c], p2s.at[c], p2r.at[c], {"tp": sib}))
        second[c].start()
    mine = [partial(tp, c) for c in range(OUT_CHUNKS)]
    for c in range(OUT_CHUNKS):
        second[c].wait_recv()
        mine[c] = mine[c] + p2_in[c].astype(F32)
    for c in range(OUT_CHUNKS):
        cross[c].wait_recv()
        out_ref[:, c * ow:(c + 1) * ow] = (mine[c] + c_in[c].astype(F32)).astype(BF16)

    for copy in to_sib + to_oth + forward + gain_copies + [halo_up, halo_down] + first + second + cross:
        copy.wait_send()
    repeat(1, n_sp, lambda r: interval_copy(r).wait_send())
    repeat(1, n_sp, lambda r: edge_copy(r).wait_send())


def per_device(
    n_sp, n_tp,
    stream, norm_gain, w_value, w_mix, w_gate, w_state, conv_taps, skip_gain, decay_rate, turn_rate,
    input_real, input_imag, read_real, read_imag, initial_state, intervals, proj_conv, proj_state,
):
    rows, width = stream.shape
    channels = w_value.shape[1]
    dirs, groups, per, group = input_real.shape
    states = dirs * groups * per
    cw, ow = width // CHUNKS, width // OUT_CHUNKS
    hbm = pl.BlockSpec(memory_space=pltpu.HBM)
    dma = lambda n: pltpu.SemaphoreType.DMA((n,))
    packed = pltpu.VMEM((rows * 8, 128), F32)
    rows_of = lambda m: jnp.swapaxes(m, 2, 3).reshape(dirs * groups * group, per)
    return pl.pallas_call(
        functools.partial(kernel, n_sp, n_tp),
        out_shape=jax.ShapeDtypeStruct((rows, width), BF16),
        in_specs=[hbm] * 18,
        out_specs=pl.BlockSpec(memory_space=pltpu.VMEM),
        scratch_shapes=[
            pltpu.VMEM((rows, width), BF16),
            pltpu.VMEM((1, width), F32),
            pltpu.VMEM(conv_taps.shape, F32),
            pltpu.VMEM((1, channels), F32),
            pltpu.VMEM((dirs * groups, per), F32),
            pltpu.VMEM((dirs * groups, per), F32),
            pltpu.VMEM((dirs * 2 * groups, per), F32),
            pltpu.SMEM((1, rows), F32),
            pltpu.VMEM((width * n_tp, 4 * channels), BF16),
            pltpu.VMEM((2 * channels, width * n_tp), BF16),
            pltpu.VMEM((2, dirs * groups * group, per), F32),
            pltpu.VMEM((2, dirs * groups * group, per), F32),
            pltpu.VMEM((n_tp, CHUNKS, rows, cw), BF16),
            pltpu.VMEM((n_tp, 1, width), F32),
            pltpu.VMEM((n_sp, 1, rows), F32),
            packed, packed, packed, packed, packed, packed, packed, packed, packed, packed,
            pltpu.VMEM((2, channels, states), BF16),
            pltpu.VMEM((2, channels, states), BF16),
            pltpu.VMEM((rows, channels), BF16),
            pltpu.VMEM((2, 16, channels), BF16),
            pltpu.VMEM((2, 8, 128), F32),
            pltpu.VMEM((n_sp, 2, 8, 128), F32),
            pltpu.VMEM((n_sp, 8, 128), F32),
            pltpu.VMEM((n_sp, 8, 128), F32),
        ] + [pltpu.VMEM((OUT_CHUNKS, rows, ow), BF16)] * 6 + [
            dma(18),
            dma(CHUNKS), dma(CHUNKS), dma(CHUNKS), dma(CHUNKS), dma(CHUNKS), dma(CHUNKS),
            dma(n_tp), dma(n_tp), dma(n_sp), dma(n_sp), dma(2), dma(2), dma(n_sp), dma(n_sp),
            dma(OUT_CHUNKS), dma(OUT_CHUNKS), dma(OUT_CHUNKS), dma(OUT_CHUNKS),
            dma(OUT_CHUNKS), dma(OUT_CHUNKS),
        ],
        compiler_params=pltpu.CompilerParams(
            collective_id=0, has_side_effects=True, vmem_limit_bytes=48 * 1024 * 1024),
    )(*(pltpu.with_memory_space_constraint(a, pltpu.HBM) for a in (
        stream, norm_gain.reshape(1, width), w_value, w_mix, w_gate, w_state, conv_taps,
        skip_gain.reshape(1, channels),
        decay_rate.reshape(dirs * groups, per), turn_rate.reshape(dirs * groups, per),
        rows_of(input_real), rows_of(input_imag),
        read_real.reshape(dirs * groups * group, per), read_imag.reshape(dirs * groups * group, per),
        initial_state.reshape(dirs * 2 * groups, per), intervals.reshape(1, rows),
        proj_conv, proj_state,
    )))


def solution(mesh):
    return jax.shard_map(
        functools.partial(per_device, mesh.shape["sp"], mesh.shape["tp"]),
        mesh=mesh,
        in_specs=(
            P("sp", "tp"), P("tp"), P(None, "tp"), P(None, "tp"), P(None, "tp"), P(None, "tp"),
            P(None, "tp"), P("tp"), P(None, "tp", None), P(None, "tp", None),
            P(None, "tp", None, None), P(None, "tp", None, None), P(None, "tp", None, None),
            P(None, "tp", None, None), P(None, None, "tp", None), P("sp"), P("tp", None),
            P("tp", None),
        ),
        out_specs=P("sp", "tp"),
        check_vma=False,
    )
```

profile of v0, /device:TPU:0, one launch (start us, length us, event | category | flops | bytes accessed | tf_op | source)
XLA Modules:
  0.0 24.3 jit_solution(9490704589748713097)
XLA Ops:
  0.0 23.7 %shard_map.172 = bf16[128,512]{1,0:T(8,128)(2,1)S(1)} custom-call(bf16[128,512]{1,0:T(8,128)(2,1)} %x_hbm.1, f32[1,512]{1,0:T(1,128)} %bitcast.21, bf16[2048,128]{1,0:T(8,128)(2,1)} %wv.1, bf16[2048,128]{1,0:T(8,128)(2,1)} %wm.1, bf16[2048,128]{1,0:T(8,128)(2,1)} %wg.1, bf16[2048,128]{1,0:T(8,128)(2,1)} %ws.1, f32[3,128]{1,0:T(4,128)} %taps_hbm.1, ...), custom_call_target="tpu_custom_call" | custom-call | tf_op jit(solution)/shard_map/pallas_call | solution.py:393
  23.7 0.7 %copy.20 = bf16[128,512]{1,0:T(8,128)(2,1)} copy(bf16[128,512]{1,0:T(8,128)(2,1)S(1)} %shard_map.172) | data formatting | bytes 262144
where the time goes:
time: 24.5 us; the launch traced here: 24.3 us
  Pallas kernels  23.7 us (97%)
  local copies, waits for them, and re-layouts  0.66 us (3%)
    pallas_call x1, Pallas kernels, per_device(): pl.pallas_call(functools.partial(kernel, n_sp, n_tp), out_shape=jax.Shape...  23.7 us
    unnamed x1, local copies, waits for them, and re-layouts  0.66 us

commit v1 on v0

v1 whole, which is shorter than its diff:
```python
import functools

import jax
import jax.numpy as jnp
from jax import lax
from jax.experimental import pallas as pl
from jax.experimental.pallas import tpu as pltpu
from jax.sharding import PartitionSpec as P

EPSILON = 1e-06
MESH = pl.DeviceIdType.MESH
F32 = jnp.float32
BF16 = jnp.bfloat16
CHUNKS = 4


def dot(a, b):
    return jnp.dot(a, b, preferred_element_type=F32)


def dot_t(a, b):
    return lax.dot_general(a, b, (((1,), (1,)), ((), ())), preferred_element_type=F32)


def half_turns(angle):
    theta = 0.5 * angle
    n = jnp.floor(theta * 0.6366197723675814 + 0.5)
    r = theta - n * 1.5703125
    r = r - n * 0.00048351287841796875
    r = r - n * 3.1385570764541626e-07
    r = r - n * 6.077100627776710e-11
    odd = (n - 2.0 * jnp.floor(0.5 * n)) > 0.5
    z = r * r
    s = r + r * z * ((-1.9515295891e-4 * z + 8.3321608736e-3) * z - 1.6666654611e-1)
    c = 1.0 - 0.5 * z + z * z * (
        (2.443315711809948e-5 * z - 1.388731625493765e-3) * z + 4.166664568298827e-2
    )
    square = jnp.where(odd, c * c, s * s)
    double = 2.0 * s * c
    return square, jnp.where(odd, -double, double)


def expm1_of(x, e):
    p = 1.0 + x * (1.0 / 7.0)
    for k in (6.0, 5.0, 4.0, 3.0, 2.0):
        p = 1.0 + x * p * (1.0 / k)
    return jnp.where(x > -0.35, x * p, e - 1.0)


def repeat(lo, hi, body):
    if hi - lo <= 16:
        for i in range(lo, hi):
            body(i)
    else:
        def step(i, carry):
            body(i)
            return carry
        lax.fori_loop(lo, hi, step, 0)


def fold(lo, hi, body, init):
    if hi - lo <= 16:
        for i in range(lo, hi):
            init = body(i, init)
        return init
    return lax.fori_loop(lo, hi, body, init)


def kernel(
    n_sp, n_tp,
    x_hbm, gain_hbm, wv, wm, wg, ws, taps_hbm, skip_hbm, decay_hbm, turn_hbm,
    inr, ini, rdr, rdi, init_hbm, iv_hbm, pc, ps,
    out_ref,
    x_ref, gain_ref, taps_ref, skip_ref, decay_ref, turn_ref, init_ref, iv_s,
    w_all, pc_v, ps_v, in_v, rd_v, x_full, gains, el_all, fr_ref, fi_ref, gr_ref, gi_ref,
    dr_ref, di_ref, hr_ref, hi_ref, kr_ref, ki_ref, k_row, d_row, p_row,
    bt_ref, rt_ref, rc_ref, cc_ref, src_ref, halo_ref, e_out, e_all,
    span_ref, wa_ref, wb_ref, p1_out, p1_in, p2_out, p2_in, c_out, c_in, acc_ref, so_ref, so_all,
    load_sem, as_sem, ar_sem, bs_sem, br_sem, fs_sem, fwr_sem, gs_sem, grv_sem,
    is_sem, ir_sem, hs_sem, hr_sem, es_sem, er_sem, ps_sem, pr_sem, ws_sem, wr_sem, ss_sem, sr_sem, greet_sem,
):
    tp, sp = lax.axis_index("tp"), lax.axis_index("sp")
    rows, width = x_hbm.shape
    channels = wv.shape[1]
    y, core = tp // 2, tp % 2
    sib = y * 2 + 1 - core
    oth = (1 - y) * 2 + core
    diag = (1 - y) * 2 + 1 - core
    cw = width // CHUNKS

    loads = {}

    def load(name, src, dst):
        copy = pltpu.make_async_copy(src, dst, load_sem.at[len(loads)])
        copy.start()
        loads[name] = copy

    def loaded(*names):
        for name in names:
            loads[name].wait()

    def near(step, act):
        for s in (-step, step):
            @pl.when((sp + s >= 0) & (sp + s < n_sp))
            def _():
                act(sp + s)

    def near_count(step):
        return jnp.where(sp - step >= 0, 1, 0) + jnp.where(sp + step < n_sp, 1, 0)

    def greet(k):
        near(1 << k, lambda where: pl.semaphore_signal(
            greet_sem.at[k], inc=1, device_id={"sp": where}, device_id_type=MESH))

    def greeted(k):
        pl.semaphore_wait(greet_sem.at[k], near_count(1 << k))

    rounds = greet_sem.shape[0]
    barrier = pltpu.get_barrier_semaphore()
    for j in range(1, n_tp):
        pl.semaphore_signal(barrier, inc=1, device_id={"tp": (tp + j) % n_tp}, device_id_type=MESH)
    near(1, lambda where: pl.semaphore_signal(
        barrier, inc=1, device_id={"sp": where}, device_id_type=MESH))
    load("x", x_hbm, x_ref)
    load("iv", iv_hbm, iv_s)
    load("decay", decay_hbm, decay_ref)
    load("turn", turn_hbm, turn_ref)
    load("init", init_hbm, init_ref)
    load("gain", gain_hbm, gain_ref)
    load("inr", inr, in_v.at[0])
    load("ini", ini, in_v.at[1])
    load("rdr", rdr, rd_v.at[0])
    load("rdi", rdi, rd_v.at[1])
    for j, w in enumerate((wv, wm, wg, ws)):
        load("w%d" % j, w, w_all.at[:, pl.ds(j * channels, channels)])
    load("taps", taps_hbm, taps_ref)
    load("skip", skip_hbm, skip_ref)
    load("pc", pc, pc_v)
    load("ps", ps.at[:, pl.ds(pl.multiple_of(tp * width, width), width)], ps_v.at[tp])
    pl.semaphore_wait(barrier, n_tp - 1 + near_count(1))
    loaded("x")

    def remote(src, dst, send, recv, where):
        return pltpu.make_async_remote_copy(
            src_ref=src, dst_ref=dst, send_sem=send, recv_sem=recv,
            device_id=where, device_id_type=MESH)

    to_sib, to_oth, forward = [], [], []
    for c in range(CHUNKS):
        piece = x_ref.at[:, pl.ds(c * cw, cw)]
        to_oth.append(remote(piece, x_full.at[tp, c], bs_sem.at[c], br_sem.at[c], {"tp": oth}))
        to_sib.append(remote(piece, x_full.at[tp, c], as_sem.at[c], ar_sem.at[c], {"tp": sib}))
        forward.append(remote(x_full.at[oth, c], x_full.at[oth, c], fs_sem.at[c], fwr_sem.at[c],
                              {"tp": sib}))
    for c in range(CHUNKS):
        to_oth[c].start()
    for c in range(CHUNKS):
        to_sib[c].start()
    gain_copies = [
        remote(gain_hbm, gains.at[tp], gs_sem.at[j], grv_sem.at[j], {"tp": (tp + j) % n_tp})
        for j in range(1, n_tp)
    ]
    for copy in gain_copies:
        copy.start()
    greet(0)
    peers = (oth, diag, sib)
    weight_copies = [
        remote(ps.at[:, pl.ds(pl.multiple_of(peer * width, width), width)], ps_v.at[tp],
               ws_sem.at[i], wr_sem.at[i], {"tp": peer})
        for i, peer in enumerate(peers)
    ]
    for copy in weight_copies:
        copy.start()

    def pass_on(c):
        to_oth[c].wait_recv()
        forward[c].start()

    sub = lax.broadcasted_iota(jnp.int32, (8, 128), 0)
    top = sub < 4

    def pack(ref):
        even = ref[pl.ds(0, 8, stride=2), :]
        odd = ref[pl.ds(1, 8, stride=2), :]
        return jnp.concatenate([even, odd], axis=1)

    loaded("iv", "decay", "turn", "init")
    decay, turn = pack(decay_ref), pack(turn_ref)
    den = decay * decay + turn * turn
    td, dd = turn / den, decay / den

    def factors(k, carry):
        iv = jnp.where(top, iv_s[0, k], iv_s[0, rows - 1 - k])
        damp = -decay * iv
        square, sine = half_turns(turn * iv)
        e = jnp.exp(damp)
        cosine = 1.0 - 2.0 * square
        f_im = e * sine
        lift = expm1_of(damp, e) * cosine - 2.0 * square
        at = pl.ds(pl.multiple_of(k * 8, 8), 8)
        fr_ref[at, :] = e * cosine
        fi_ref[at, :] = f_im
        gr_ref[at, :] = td * f_im - dd * lift
        gi_ref[at, :] = -(dd * f_im + td * lift)
        return carry

    lax.fori_loop(0, rows, factors, 0, unroll=4)
    greeted(0)
    if rounds > 1:
        greet(1)

    def put(ref, k, value):
        ref[pl.ds(pl.multiple_of(k * 8, 8), 4), :] = value[:4]
        ref[pl.ds(pl.multiple_of((rows - 1 - k) * 8, 8) + 4, 4), :] = value[4:]

    def chain(k, carry):
        ar, ai, br, bi = carry
        at = pl.ds(pl.multiple_of(k * 8, 8), 8)
        back = pl.ds(pl.multiple_of((rows - 1 - k) * 8, 8), 8)
        fr, fi = fr_ref[at, :], fi_ref[at, :]
        ar, ai = fr * ar - fi * ai, fr * ai + fi * ar
        put(hr_ref, k, ar)
        put(hi_ref, k, ai)
        gr, gi = gr_ref[back, :], gi_ref[back, :]
        put(kr_ref, rows - 1 - k, gr * br - gi * bi)
        put(ki_ref, rows - 1 - k, gr * bi + gi * br)
        fr, fi = fr_ref[back, :], fi_ref[back, :]
        return ar, ai, fr * br - fi * bi, fr * bi + fi * br

    one, zero = jnp.ones((8, 128), F32), jnp.zeros((8, 128), F32)
    lax.fori_loop(0, rows, chain, (one, zero, one, zero), unroll=4)
    pass_on(0)
    for part, (k_ref, h_ref) in enumerate(((kr_ref, hr_ref), (ki_ref, hi_ref))):
        for j in range(8):
            lanes = slice(j * 128, (j + 1) * 128)
            k_row[part, :, lanes] = k_ref[pl.ds(j, rows, stride=8), :]
            p_row[part, :, lanes] = h_ref[pl.ds(j, rows, stride=8), :].astype(BF16)
    pass_on(1)
    if rounds > 1:
        greeted(1)
    for k in range(2, rounds):
        greet(k)
        if k < rounds - 1:
            greeted(k)

    loaded("inr", "ini", "rdr", "rdi")
    states = bt_ref.shape[2]
    per = rd_v.shape[2]
    half = states // 2
    group = channels * per // half
    spread = (lax.broadcasted_iota(jnp.int32, (per, half), 1) % per
              == lax.broadcasted_iota(jnp.int32, (per, half), 0)).astype(BF16)
    keep = ((lax.broadcasted_iota(jnp.int32, (channels, half), 1) // per)
            == (lax.broadcasted_iota(jnp.int32, (channels, half), 0) // group))
    left = lax.broadcasted_iota(jnp.int32, (group, 2 * per), 1) < per
    for part in range(2):
        for d in range(2):
            at, to = pl.ds(d * channels, channels), pl.ds(d * half, half)
            wide = dot(in_v[part, at, :].astype(BF16), spread)
            bt_ref[part, :, to] = jnp.where(keep, wide, 0.0).astype(BF16)
            wide = dot(rd_v[part, at, :].astype(BF16), spread)
            if part:
                wide = -wide
            rt_ref[part, :, to] = jnp.where(keep, wide, 0.0).astype(BF16)
            for g in range(channels // group):
                narrow = rd_v[part, pl.ds(d * channels + g * group, group), :]
                both = jnp.concatenate([narrow, narrow], axis=1)
                cc_ref[part, d, g] = jnp.where(left if g % 2 == 0 else ~left, both, 0.0)
    rc_ref[...] = jnp.zeros_like(rc_ref)

    pass_on(2)
    loaded("gain", "w0", "w1", "w2", "w3")
    for copy in gain_copies:
        copy.wait_recv()

    def project(value, gain, first):
        wide = value.astype(F32)
        scaled = (wide * gain).astype(BF16)
        k = value.shape[1]
        term = dot(scaled, w_all[pl.ds(pl.multiple_of(first, k), k), :])
        return term, jnp.sum(wide * wide, axis=1, keepdims=True)

    projected = jnp.zeros((rows, 4 * channels), F32)
    squares = jnp.zeros((rows, 1), F32)
    t, s = project(x_ref[...], gain_ref[...], tp * width)
    projected, squares = projected + t, squares + s

    def whole(owner, projected, squares):
        value = jnp.concatenate([x_full[owner, c] for c in range(CHUNKS)], axis=1)
        t, s = project(value, gains[owner], owner * width)
        return projected + t, squares + s

    for c in range(CHUNKS):
        to_sib[c].wait_recv()
    projected, squares = whole(sib, projected, squares)
    pass_on(3)
    projected, squares = whole(oth, projected, squares)
    if rounds > 2:
        greeted(rounds - 1)

    def interval_copy(r):
        return remote(iv_hbm, el_all.at[r], is_sem.at[r], ir_sem.at[r], {"sp": (sp + r) % n_sp})

    repeat(1, n_sp, lambda r: interval_copy(r).start())
    for c in range(CHUNKS):
        forward[c].wait_recv()
        t, s = project(x_full[diag, c], gains[diag][:, c * cw:(c + 1) * cw], diag * width + c * cw)
        projected, squares = projected + t, squares + s
    projected = projected * lax.rsqrt(squares / (width * n_tp) + EPSILON)
    state_input = projected[:, 3 * channels:].astype(BF16)
    conv_value = projected[:, :channels].astype(BF16).astype(F32)
    conv_mix = projected[:, channels:2 * channels].astype(BF16).astype(F32)
    conv_gate = projected[:, 2 * channels:3 * channels].astype(BF16).astype(F32)
    src_ref[...] = (conv_mix * conv_value).astype(BF16)

    for j in range(4):
        lanes = slice(j * 256, (j + 1) * 256)
        dr = dot(state_input, bt_ref[0, :, lanes])
        di = dot(state_input, bt_ref[1, :, lanes])
        d_row[0, :, lanes] = dr
        d_row[1, :, lanes] = di
        kr, ki = k_row[0, :, lanes], k_row[1, :, lanes]
        er = jnp.sum(kr * dr - ki * di, axis=0, keepdims=True)
        ei = jnp.sum(kr * di + ki * dr, axis=0, keepdims=True)
        for h in range(2):
            q = (j % 2) * 2 + h
            e_out[j // 2, q:q + 1, :] = er[:, h * 128:(h + 1) * 128]
            e_out[j // 2, 4 + q:5 + q, :] = ei[:, h * 128:(h + 1) * 128]


    def edge_copy(r):
        return remote(e_out.at[jnp.where(sp + r < n_sp, 0, 1)], e_all.at[r], es_sem.at[r],
                      er_sem.at[r], {"sp": (sp + r) % n_sp})

    halo_up = remote(src_ref.at[pl.ds(rows - 16, 16)], halo_ref.at[0], hs_sem.at[0], hr_sem.at[0],
                     {"sp": (sp + 1) % n_sp})
    halo_down = remote(src_ref.at[pl.ds(0, 16)], halo_ref.at[1], hs_sem.at[1], hr_sem.at[1],
                       {"sp": (sp + n_sp - 1) % n_sp})
    repeat(1, n_sp, lambda r: edge_copy(r).start())
    not_first, not_last = sp > 0, sp < n_sp - 1
    pl.when(not_last)(halo_up.start)
    pl.when(not_first)(halo_down.start)

    for part, ref in ((0, dr_ref), (1, di_ref)):
        for j in range(8):
            ref[pl.ds(j, rows, stride=8), :] = d_row[part, :, j * 128:(j + 1) * 128]


    def local(k, carry):
        hr, hi = carry
        at = pl.ds(pl.multiple_of(k * 8, 8), 8)
        back = pl.ds(pl.multiple_of((rows - 1 - k) * 8, 8), 8)
        dr = jnp.where(top, dr_ref[at, :], dr_ref[back, :])
        di = jnp.where(top, di_ref[at, :], di_ref[back, :])
        gr, gi = gr_ref[at, :], gi_ref[at, :]
        fr, fi = fr_ref[at, :], fi_ref[at, :]
        pr = gr * dr - gi * di
        pi = gr * di + gi * dr
        hr, hi = fr * hr + (pr - fi * hi), fr * hi + (pi + fi * hr)
        put(hr_ref, k, hr)
        put(hi_ref, k, hi)
        return hr, hi

    lax.fori_loop(0, rows, local, (zero, zero), unroll=8)
    loaded("taps", "skip", "pc", "ps")
    response = state_input.astype(F32) * skip_ref[...]
    for part, ref in ((0, hr_ref), (1, hi_ref)):
        history = jnp.concatenate(
            [ref[pl.ds(j, rows, stride=8), :].astype(BF16) for j in range(8)], axis=1)
        response = response + dot_t(history, rt_ref[part])

    pl.when(not_first)(halo_up.wait_recv)
    pl.when(not_last)(halo_down.wait_recv)
    source = src_ref[...].astype(F32)
    line = lax.broadcasted_iota(jnp.int32, (rows, channels), 0)
    before = jnp.where(not_first, halo_ref[0].astype(F32)[15:16, :], 0.0)
    after = jnp.where(not_last, halo_ref[1].astype(F32)[0:1, :], 0.0)
    previous = jnp.where(line == 0, before, pltpu.roll(source, 1, 0))
    following = jnp.where(line == rows - 1, after, pltpu.roll(source, rows - 1, 0))
    filtered = taps_ref[0:1, :] * previous + taps_ref[1:2, :] * source + taps_ref[2:3, :] * following
    conv_out = (conv_gate * filtered).astype(BF16)

    def partial(owner):
        return dot(conv_out, pc_v[:, pl.ds(pl.multiple_of(owner * width, width), width)])

    p1_out[...] = partial(diag).astype(BF16)
    first = remote(p1_out, p1_in, ps_sem.at[0], pr_sem.at[0], {"tp": sib})
    first.start()
    p2_out[...] = partial(sib).astype(BF16)
    second = remote(p2_out, p2_in, ps_sem.at[1], pr_sem.at[1], {"tp": sib})
    second.start()
    acc_ref[...] = partial(oth)

    repeat(1, n_sp, lambda r: interval_copy(r).wait_recv())

    def both_of(full, d):
        return jnp.concatenate([full[d * 4:d * 4 + 4], full[d * 4:d * 4 + 4]], axis=0)

    def init_of(d):
        parts = [
            jnp.concatenate([init_ref[pl.ds(d * 16 + part * 8, 4, stride=2), :],
                             init_ref[pl.ds(d * 16 + part * 8 + 1, 4, stride=2), :]], axis=1)
            for part in range(2)
        ]
        return jnp.concatenate(parts, axis=0)

    decays = [both_of(decay, d) for d in range(2)]
    turns = [both_of(turn, d) for d in range(2)]

    def weight(damping, turning, span):
        square, sine = half_turns(turning * span)
        e = jnp.exp(-damping * span)
        return e * (1.0 - 2.0 * square), jnp.where(top, -e * sine, e * sine)

    def apply(w, tile):
        return w[0] * tile + w[1] * pltpu.roll(tile, 4, 0)

    def elapsed(r):
        return jnp.sum(el_all[r], axis=1, keepdims=True)

    none = jnp.zeros((1, 1), F32)

    def ahead(r, carry):
        total, inside = carry
        span_ref[r] = jnp.broadcast_to(total, (1, 128))
        step = elapsed(r)
        return total + step, inside + step * jnp.where(sp - r >= 0, 1.0, 0.0)

    total, inside = fold(1, n_sp, ahead, (none, none))

    def behind(i, total):
        r = n_sp - i
        mine = sp - r >= 0
        span = jnp.where(mine, span_ref[r], jnp.broadcast_to(total, (1, 128)))
        w = weight(jnp.where(mine, decays[0], decays[1]), jnp.where(mine, turns[0], turns[1]), span)
        wa_ref[r] = w[0]
        wb_ref[r] = w[1]
        return total + elapsed(r)

    fold(1, n_sp, behind, none)
    outside = none

    def beyond(r, acc):
        return acc + elapsed(r) * jnp.where(sp - r >= 0, 0.0, 1.0)

    outside = fold(1, n_sp, beyond, none)
    h0 = apply(weight(decays[0], turns[0], inside), init_of(0))
    h1 = apply(weight(decays[1], turns[1], outside), init_of(1))

    first.wait_recv()
    c_out[...] = (acc_ref[...] + p1_in[...].astype(F32)).astype(BF16)
    cross = remote(c_out, c_in, ps_sem.at[2], pr_sem.at[2], {"tp": oth})
    cross.start()
    mine = partial(tp)
    second.wait_recv()
    acc_ref[...] = mine + p2_in[...].astype(F32)

    repeat(1, n_sp, lambda r: edge_copy(r).wait_recv())

    def combine(r, carry):
        h0, h1 = carry
        moved = apply((wa_ref[r], wb_ref[r]), e_all[r])
        mine = sp - r >= 0
        return h0 + jnp.where(mine, moved, 0.0), h1 + jnp.where(mine, 0.0, moved)

    entering = fold(1, n_sp, combine, (h0, h1))
    for d in range(2):
        for g in range(channels // group):
            q = g // 2
            hr, hi = entering[d][q:q + 1, :], entering[d][4 + q:5 + q, :]
            cr_, ci_ = cc_ref[0, d, g], cc_ref[1, d, g]
            at, lanes = pl.ds(g * group, group), pl.ds(d * half + q * 128, 128)
            rc_ref[0, at, lanes] = (cr_ * hr - ci_ * hi).astype(BF16)
            rc_ref[1, at, lanes] = (-(cr_ * hi + ci_ * hr)).astype(BF16)
    for part in range(2):
        response = response + dot_t(p_row[part], rc_ref[part])
    inner = 0.7978845608028654 * (response + 0.044715 * (response * response * response))
    state_out = (0.5 * response * (1.0 + jnp.tanh(inner))).astype(BF16)
    so_ref[...] = state_out
    state_copies = [
        remote(so_ref, so_all.at[tp], ss_sem.at[i], sr_sem.at[i], {"tp": peer})
        for i, peer in enumerate(peers)
    ]
    for copy in state_copies:
        copy.start()
    total = acc_ref[...] + dot(state_out, ps_v[tp])
    for copy in weight_copies:
        copy.wait_recv()
    cross.wait_recv()
    total = total + c_in[...].astype(F32)
    for i in (2, 0, 1):
        state_copies[i].wait_recv()
        total = total + dot(so_all[peers[i]], ps_v[peers[i]])
    out_ref[...] = total.astype(BF16)

    pl.when(not_last)(halo_up.wait_send)
    pl.when(not_first)(halo_down.wait_send)
    for copy in (to_sib + to_oth + forward + gain_copies + weight_copies + state_copies
                 + [first, second, cross]):
        copy.wait_send()
    repeat(1, n_sp, lambda r: interval_copy(r).wait_send())
    repeat(1, n_sp, lambda r: edge_copy(r).wait_send())


def per_device(
    n_sp, n_tp,
    stream, norm_gain, w_value, w_mix, w_gate, w_state, conv_taps, skip_gain, decay_rate, turn_rate,
    input_real, input_imag, read_real, read_imag, initial_state, intervals, proj_conv, proj_state,
):
    rows, width = stream.shape
    channels = w_value.shape[1]
    dirs, groups, per, group = input_real.shape
    states = dirs * groups * per
    cw = width // CHUNKS
    hbm = pl.BlockSpec(memory_space=pltpu.HBM)
    dma = lambda n: pltpu.SemaphoreType.DMA((n,))
    packed = pltpu.VMEM((rows * 8, 128), F32)
    rows_of = lambda m: jnp.swapaxes(m, 2, 3).reshape(dirs * groups * group, per)
    return pl.pallas_call(
        functools.partial(kernel, n_sp, n_tp),
        out_shape=jax.ShapeDtypeStruct((rows, width), BF16),
        in_specs=[hbm] * 18,
        out_specs=pl.BlockSpec(memory_space=pltpu.VMEM),
        scratch_shapes=[
            pltpu.VMEM((rows, width), BF16),
            pltpu.VMEM((1, width), F32),
            pltpu.VMEM(conv_taps.shape, F32),
            pltpu.VMEM((1, channels), F32),
            pltpu.VMEM((dirs * groups, per), F32),
            pltpu.VMEM((dirs * groups, per), F32),
            pltpu.VMEM((dirs * 2 * groups, per), F32),
            pltpu.SMEM((1, rows), F32),
            pltpu.VMEM((width * n_tp, 4 * channels), BF16),
            pltpu.VMEM((channels, width * n_tp), BF16),
            pltpu.VMEM((n_tp, channels, width), BF16),
            pltpu.VMEM((2, dirs * groups * group, per), F32),
            pltpu.VMEM((2, dirs * groups * group, per), F32),
            pltpu.VMEM((n_tp, CHUNKS, rows, cw), BF16),
            pltpu.VMEM((n_tp, 1, width), F32),
            pltpu.VMEM((n_sp, 1, rows), F32),
            packed, packed, packed, packed, packed, packed, packed, packed, packed, packed,
            pltpu.VMEM((2, rows, states), F32),
            pltpu.VMEM((2, rows, states), F32),
            pltpu.VMEM((2, rows, states), BF16),
            pltpu.VMEM((2, channels, states), BF16),
            pltpu.VMEM((2, channels, states), BF16),
            pltpu.VMEM((2, channels, states), BF16),
            pltpu.VMEM((2, dirs, groups, group, 2 * per), F32),
            pltpu.VMEM((rows, channels), BF16),
            pltpu.VMEM((2, 16, channels), BF16),
            pltpu.VMEM((2, 8, 128), F32),
            pltpu.VMEM((n_sp, 8, 128), F32),
            pltpu.VMEM((n_sp, 1, 128), F32),
            pltpu.VMEM((n_sp, 8, 128), F32),
            pltpu.VMEM((n_sp, 8, 128), F32),
        ] + [pltpu.VMEM((rows, width), BF16)] * 6 + [
            pltpu.VMEM((rows, width), F32),
            pltpu.VMEM((rows, channels), BF16),
            pltpu.VMEM((n_tp, rows, channels), BF16),
            dma(18),
            dma(CHUNKS), dma(CHUNKS), dma(CHUNKS), dma(CHUNKS), dma(CHUNKS), dma(CHUNKS),
            dma(n_tp), dma(n_tp), dma(n_sp), dma(n_sp), dma(2), dma(2), dma(n_sp), dma(n_sp),
            dma(3), dma(3), dma(3), dma(3), dma(3), dma(3),
            pltpu.SemaphoreType.REGULAR((max(2, (n_sp - 1).bit_length()),)),
        ],
        compiler_params=pltpu.CompilerParams(
            collective_id=0, has_side_effects=True, vmem_limit_bytes=48 * 1024 * 1024),
    )(*(pltpu.with_memory_space_constraint(a, pltpu.HBM) for a in (
        stream, norm_gain.reshape(1, width), w_value, w_mix, w_gate, w_state, conv_taps,
        skip_gain.reshape(1, channels),
        decay_rate.reshape(dirs * groups, per), turn_rate.reshape(dirs * groups, per),
        rows_of(input_real), rows_of(input_imag),
        read_real.reshape(dirs * groups * group, per), read_imag.reshape(dirs * groups * group, per),
        initial_state.reshape(dirs * 2 * groups, per), intervals.reshape(1, rows),
        proj_conv, proj_state,
    )))


def solution(mesh):
    return jax.shard_map(
        functools.partial(per_device, mesh.shape["sp"], mesh.shape["tp"]),
        mesh=mesh,
        in_specs=(
            P("sp", "tp"), P("tp"), P(None, "tp"), P(None, "tp"), P(None, "tp"), P(None, "tp"),
            P(None, "tp"), P("tp"), P(None, "tp", None), P(None, "tp", None),
            P(None, "tp", None, None), P(None, "tp", None, None), P(None, "tp", None, None),
            P(None, "tp", None, None), P(None, None, "tp", None), P("sp"), P("tp", None),
            P("tp", None),
        ),
        out_specs=P("sp", "tp"),
        check_vma=False,
    )
```

time: 24.5 us -> 22.9 us (0.935)
  Pallas kernels: 23.7 us -> 22 us
    pallas_call x1, Pallas kernels: 23.7 us -> 22 us  [per_device(): pl.pallas_call(functools.partial(kernel, n_sp, n_tp), out_shape=jax.Shape...]
where the time goes in v1:
time: 22.9 us; the launch traced here: 22.7 us
  Pallas kernels  22 us (96%)
  local copies, waits for them, and re-layouts  0.66 us (3%)
    pallas_call x1, Pallas kernels, per_device(): pl.pallas_call(functools.partial(kernel, n_sp, n_tp), out_shape=jax.Shape...  22 us
    unnamed x1, local copies, waits for them, and re-layouts  0.66 us

profile of v1, /device:TPU:0, one launch (start us, length us, event | category | flops | bytes accessed | tf_op | source)
XLA Modules:
  0.0 22.7 jit_solution(10792701093295705630)
XLA Ops:
  0.0 22.0 %shard_map.172 = bf16[128,512]{1,0:T(8,128)(2,1)S(1)} custom-call(bf16[128,512]{1,0:T(8,128)(2,1)} %x_hbm.1, f32[1,512]{1,0:T(1,128)} %bitcast.21, bf16[2048,128]{1,0:T(8,128)(2,1)} %wv.1, bf16[2048,128]{1,0:T(8,128)(2,1)} %wm.1, bf16[2048,128]{1,0:T(8,128)(2,1)} %wg.1, bf16[2048,128]{1,0:T(8,128)(2,1)} %ws.1, f32[3,128]{1,0:T(4,128)} %taps_hbm.1, ...), custom_call_target="tpu_custom_call" | custom-call | tf_op jit(solution)/shard_map/pallas_call | solution.py:519
  22.1 0.7 %copy.20 = bf16[128,512]{1,0:T(8,128)(2,1)} copy(bf16[128,512]{1,0:T(8,128)(2,1)S(1)} %shard_map.172) | data formatting | bytes 262144

commit v2 on v1

--- a/solution.py
+++ b/solution.py
@@ -71,13 +71,14 @@
     x_hbm, gain_hbm, wv, wm, wg, ws, taps_hbm, skip_hbm, decay_hbm, turn_hbm,
     inr, ini, rdr, rdi, init_hbm, iv_hbm, pc, ps,
     out_ref,
-    x_ref, gain_ref, taps_ref, skip_ref, decay_ref, turn_ref, init_ref, iv_s,
+    x_ref, gain_ref, taps_ref, skip_ref, decay_ref, turn_ref, init_ref, iv_s, iv_v,
     w_all, pc_v, ps_v, in_v, rd_v, x_full, gains, el_all, fr_ref, fi_ref, gr_ref, gi_ref,
     dr_ref, di_ref, hr_ref, hi_ref, kr_ref, ki_ref, k_row, d_row, p_row,
-    bt_ref, rt_ref, rc_ref, cc_ref, src_ref, halo_ref, e_out, e_all,
-    span_ref, wa_ref, wb_ref, p1_out, p1_in, p2_out, p2_in, c_out, c_in, acc_ref, so_ref, so_all,
+    bt_ref, rt_ref, rc_ref, cq_ref, src_ref, halo_ref, e_out, e_all,
+    span_ref, wa_ref, wb_ref, p1_out, p1_in, p2_out, p2_in, c_out, c_in, acc_ref, so_ref, so_in,
+    rp_out, rp_in, kept_ref,
     load_sem, as_sem, ar_sem, bs_sem, br_sem, fs_sem, fwr_sem, gs_sem, grv_sem,
-    is_sem, ir_sem, hs_sem, hr_sem, es_sem, er_sem, ps_sem, pr_sem, ws_sem, wr_sem, ss_sem, sr_sem, greet_sem,
+    is_sem, ir_sem, hs_sem, hr_sem, es_sem, er_sem, ps_sem, pr_sem, ws_sem, wr_sem, ss_sem, sr_sem, os_sem, or_sem, greet_sem,
 ):
     tp, sp = lax.axis_index("tp"), lax.axis_index("sp")
     rows, width = x_hbm.shape
@@ -123,9 +124,10 @@
         barrier, inc=1, device_id={"sp": where}, device_id_type=MESH))
     load("x", x_hbm, x_ref)
     load("iv", iv_hbm, iv_s)
-    load("decay", decay_hbm, decay_ref)
-    load("turn", turn_hbm, turn_ref)
-    load("init", init_hbm, init_ref)
+    load("ivv", iv_hbm, iv_v)
+    load("decay", decay_hbm, decay_ref.at[0])
+    load("turn", turn_hbm, turn_ref.at[0])
+    load("init", init_hbm, init_ref.at[0])
     load("gain", gain_hbm, gain_ref)
     load("inr", inr, in_v.at[0])
     load("ini", ini, in_v.at[1])
@@ -136,7 +138,7 @@
     load("taps", taps_hbm, taps_ref)
     load("skip", skip_hbm, skip_ref)
     load("pc", pc, pc_v)
-    load("ps", ps.at[:, pl.ds(pl.multiple_of(tp * width, width), width)], ps_v.at[tp])
+    load("ps", ps.at[:, pl.ds(pl.multiple_of(tp * width, width), width)], ps_v.at[pl.ds(0, channels)])
     pl.semaphore_wait(barrier, n_tp - 1 + near_count(1))
     loaded("x")
 
@@ -163,14 +165,35 @@
     for copy in gain_copies:
         copy.start()
     greet(0)
-    peers = (oth, diag, sib)
+    part_rows = channels // 2
+    my_part = pl.multiple_of((sp % 2) * part_rows, part_rows)
+    twin = sp + 1 - 2 * (sp % 2)
+
+    def columns(owner):
+        return pl.ds(pl.multiple_of(owner * width, width), width)
+
+    def slot(pos):
+        return ps_v.at[pl.ds(pos * channels + my_part, part_rows)]
+
     weight_copies = [
-        remote(ps.at[:, pl.ds(pl.multiple_of(peer * width, width), width)], ps_v.at[tp],
-               ws_sem.at[i], wr_sem.at[i], {"tp": peer})
-        for i, peer in enumerate(peers)
+        remote(ps.at[:, columns(sib)], ps_v.at[pl.ds(2 * channels, channels)],
+               ws_sem.at[0], wr_sem.at[0], {"tp": sib}),
+        remote(ps.at[pl.ds(my_part, part_rows), columns(oth)], slot(1), ws_sem.at[1], wr_sem.at[1],
+               {"tp": oth}),
+        remote(ps.at[pl.ds(my_part, part_rows), columns(diag)], slot(3), ws_sem.at[2], wr_sem.at[2],
+               {"tp": diag}),
     ]
-    for copy in weight_copies:
-        copy.start()
+    weight_forward = [
+        remote(slot(pos), slot(pos), ws_sem.at[3 + i], wr_sem.at[3 + i], {"sp": twin})
+        for i, pos in enumerate((1, 3))
+    ]
+    other_copies = [
+        remote(src, dst, os_sem.at[i], or_sem.at[i], {"tp": oth})
+        for i, (src, dst) in enumerate((
+            (decay_hbm, decay_ref.at[1]), (turn_hbm, turn_ref.at[1]), (init_hbm, init_ref.at[1]),
+            (cq_ref.at[0], cq_ref.at[1])))
+    ]
+    rest_copy = remote(rp_out, rp_in, os_sem.at[4], or_sem.at[4], {"tp": oth})
 
     def pass_on(c):
         to_oth[c].wait_recv()
@@ -185,7 +208,7 @@
         return jnp.concatenate([even, odd], axis=1)
 
     loaded("iv", "decay", "turn", "init")
-    decay, turn = pack(decay_ref), pack(turn_ref)
+    decay, turn = pack(decay_ref.at[0]), pack(turn_ref.at[0])
     den = decay * decay + turn * turn
     td, dd = turn / den, decay / den
 
@@ -204,10 +227,11 @@
         gi_ref[at, :] = -(dd * f_im + td * lift)
         return carry
 
-    lax.fori_loop(0, rows, factors, 0, unroll=4)
+    lax.fori_loop(0, 3 * rows // 4, factors, 0, unroll=4)
     greeted(0)
     if rounds > 1:
         greet(1)
+    lax.fori_loop(3 * rows // 4, rows, factors, 0, unroll=4)
 
     def put(ref, k, value):
         ref[pl.ds(pl.multiple_of(k * 8, 8), 4), :] = value[:4]
@@ -229,19 +253,23 @@
 
     one, zero = jnp.ones((8, 128), F32), jnp.zeros((8, 128), F32)
     lax.fori_loop(0, rows, chain, (one, zero, one, zero), unroll=4)
-    pass_on(0)
-    for part, (k_ref, h_ref) in enumerate(((kr_ref, hr_ref), (ki_ref, hi_ref))):
-        for j in range(8):
-            lanes = slice(j * 128, (j + 1) * 128)
-            k_row[part, :, lanes] = k_ref[pl.ds(j, rows, stride=8), :]
-            p_row[part, :, lanes] = h_ref[pl.ds(j, rows, stride=8), :].astype(BF16)
-    pass_on(1)
     if rounds > 1:
         greeted(1)
     for k in range(2, rounds):
         greet(k)
         if k < rounds - 1:
             greeted(k)
+    pass_on(0)
+    for part, (k_ref, h_ref) in enumerate(((kr_ref, hr_ref), (ki_ref, hi_ref))):
+        for j in range(8):
+            lanes = slice(j * 128, (j + 1) * 128)
+            k_row[part, :, lanes] = k_ref[pl.ds(j, rows, stride=8), :]
+            p_row[0, :, pl.ds(part * bt_ref.shape[2] + j * 128, 128)] = h_ref[pl.ds(j, rows, stride=8), :].astype(BF16)
+    pass_on(1)
+    for copy in to_oth:
+        copy.wait_send()
+    for copy in weight_copies:
+        copy.start()
 
     loaded("inr", "ini", "rdr", "rdi")
     states = bt_ref.shape[2]
@@ -262,13 +290,14 @@
             if part:
                 wide = -wide
             rt_ref[part, :, to] = jnp.where(keep, wide, 0.0).astype(BF16)
-            for g in range(channels // group):
-                narrow = rd_v[part, pl.ds(d * channels + g * group, group), :]
-                both = jnp.concatenate([narrow, narrow], axis=1)
-                cc_ref[part, d, g] = jnp.where(left if g % 2 == 0 else ~left, both, 0.0)
+            for q in range(channels // group // 2):
+                pair = [rd_v[part, pl.ds(d * channels + g * group, group), :] for g in (2 * q, 2 * q + 1)]
+                cq_ref[0, part, d, q] = jnp.concatenate(pair, axis=1).astype(BF16)
     rc_ref[...] = jnp.zeros_like(rc_ref)
 
     pass_on(2)
+    for copy in other_copies:
+        copy.start()
     loaded("gain", "w0", "w1", "w2", "w3")
     for copy in gain_copies:
         copy.wait_recv()
@@ -328,18 +357,64 @@
             e_out[j // 2, 4 + q:5 + q, :] = ei[:, h * 128:(h + 1) * 128]
 
 
-    def edge_copy(r):
-        return remote(e_out.at[jnp.where(sp + r < n_sp, 0, 1)], e_all.at[r], es_sem.at[r],
-                      er_sem.at[r], {"sp": (sp + r) % n_sp})
+    def edge_copy(r, s):
+        return remote(e_out.at[jnp.where(sp + r < n_sp, 0, 1)], e_all.at[s, r], es_sem.at[s, r],
+                      er_sem.at[s, r], {"sp": (sp + r) % n_sp, "tp": oth if s else tp})
+
+    def edges(act):
+        def at(r):
+            act(edge_copy(r, 0))
+            act(edge_copy(r, 1))
+        repeat(1, n_sp, at)
 
     halo_up = remote(src_ref.at[pl.ds(rows - 16, 16)], halo_ref.at[0], hs_sem.at[0], hr_sem.at[0],
                      {"sp": (sp + 1) % n_sp})
     halo_down = remote(src_ref.at[pl.ds(0, 16)], halo_ref.at[1], hs_sem.at[1], hr_sem.at[1],
                        {"sp": (sp + n_sp - 1) % n_sp})
-    repeat(1, n_sp, lambda r: edge_copy(r).start())
+    edges(lambda copy: copy.start())
     not_first, not_last = sp > 0, sp < n_sp - 1
     pl.when(not_last)(halo_up.start)
     pl.when(not_first)(halo_down.start)
+
+    loaded("taps", "skip", "pc", "ps")
+    edge = 16
+    inner_rows = rows - 2 * edge
+    pieces = (pl.ds(0, inner_rows), pl.ds(inner_rows, 2 * edge))
+    source = src_ref[...].astype(F32)
+    line = lax.broadcasted_iota(jnp.int32, (rows, channels), 0)
+    previous = jnp.where(line == 0, 0.0, pltpu.roll(source, 1, 0))
+    following = jnp.where(line == rows - 1, 0.0, pltpu.roll(source, rows - 1, 0))
+    filtered = taps_ref[0:1, :] * previous + taps_ref[1:2, :] * source + taps_ref[2:3, :] * following
+    conv_out = (conv_gate * filtered).astype(BF16)[edge:rows - edge]
+
+    def ends(a):
+        return jnp.concatenate([a[:edge], a[rows - edge:]], axis=0)
+
+    end_gate, end_filtered = ends(conv_gate), ends(filtered)
+
+    def products(branch, i):
+        at = pieces[i]
+        copies = [
+            remote(p1_out.at[at], p1_in.at[at], ps_sem.at[3 * i], pr_sem.at[3 * i], {"tp": sib}),
+            remote(p2_out.at[at], p2_in.at[at], ps_sem.at[3 * i + 1], pr_sem.at[3 * i + 1], {"tp": sib}),
+            remote(c_out.at[at], c_in.at[at], ps_sem.at[3 * i + 2], pr_sem.at[3 * i + 2], {"tp": oth}),
+        ]
+        p1_out[at, :] = dot(branch, pc_v[:, columns(diag)]).astype(BF16)
+        copies[0].start()
+        p2_out[at, :] = dot(branch, pc_v[:, columns(sib)]).astype(BF16)
+        copies[1].start()
+        kept = dot(branch, pc_v[:, columns(oth)])
+        acc_ref[at, :] = dot(branch, pc_v[:, columns(tp)])
+        return copies, kept
+
+    def crossing(copies, kept, i):
+        at = pieces[i]
+        copies[0].wait_recv()
+        c_out[at, :] = (kept + p1_in[at, :].astype(F32)).astype(BF16)
+        copies[2].start()
+
+    conv_a, kept = products(conv_out, 0)
+    kept_ref[...] = kept
 
     for part, ref in ((0, dr_ref), (1, di_ref)):
         for j in range(8):
@@ -362,50 +437,60 @@
         return hr, hi
 
     lax.fori_loop(0, rows, local, (zero, zero), unroll=8)
-    loaded("taps", "skip", "pc", "ps")
     response = state_input.astype(F32) * skip_ref[...]
     for part, ref in ((0, hr_ref), (1, hi_ref)):
         history = jnp.concatenate(
             [ref[pl.ds(j, rows, stride=8), :].astype(BF16) for j in range(8)], axis=1)
         response = response + dot_t(history, rt_ref[part])
 
+    rp_out[...] = response.astype(BF16)
+    rest_copy.start()
+    crossing(conv_a, kept_ref[...], 0)
+    for copy in weight_copies:
+        copy.wait_recv()
+    for copy in weight_forward:
+        copy.start()
     pl.when(not_first)(halo_up.wait_recv)
     pl.when(not_last)(halo_down.wait_recv)
-    source = src_ref[...].astype(F32)
-    line = lax.broadcasted_iota(jnp.int32, (rows, channels), 0)
-    before = jnp.where(not_first, halo_ref[0].astype(F32)[15:16, :], 0.0)
-    after = jnp.where(not_last, halo_ref[1].astype(F32)[0:1, :], 0.0)
-    previous = jnp.where(line == 0, before, pltpu.roll(source, 1, 0))
-    following = jnp.where(line == rows - 1, after, pltpu.roll(source, rows - 1, 0))
-    filtered = taps_ref[0:1, :] * previous + taps_ref[1:2, :] * source + taps_ref[2:3, :] * following
-    conv_out = (conv_gate * filtered).astype(BF16)
-
-    def partial(owner):
-        return dot(conv_out, pc_v[:, pl.ds(pl.multiple_of(owner * width, width), width)])
-
-    p1_out[...] = partial(diag).astype(BF16)
-    first = remote(p1_out, p1_in, ps_sem.at[0], pr_sem.at[0], {"tp": sib})
-    first.start()
-    p2_out[...] = partial(sib).astype(BF16)
-    second = remote(p2_out, p2_in, ps_sem.at[1], pr_sem.at[1], {"tp": sib})
-    second.start()
-    acc_ref[...] = partial(oth)
+    before = jnp.where(not_first, halo_ref[0].astype(F32)[15:16, :], 0.0) * taps_ref[0:1, :]
+    after = jnp.where(not_last, halo_ref[1].astype(F32)[0:1, :], 0.0) * taps_ref[2:3, :]
+    end_line = lax.broadcasted_iota(jnp.int32, (2 * edge, channels), 0)
+    end_filtered = end_filtered + jnp.where(
+        end_line == 0, before, jnp.where(end_line == 2 * edge - 1, after, 0.0))
+    conv_b, kept_b = products((end_gate * end_filtered).astype(BF16), 1)
+
+    for copy in other_copies:
+        copy.wait_recv()
+    decay_2, turn_2 = pack(decay_ref.at[1]), pack(turn_ref.at[1])
+    at_t = lax.broadcasted_iota(jnp.int32, (rows, rows), 0)
+    at_s = lax.broadcasted_iota(jnp.int32, (rows, rows), 1)
+    loaded("ivv")
+    steps = iv_v[...]
+    reach = (jnp.sum(jnp.where(at_s <= at_t, steps, 0.0), axis=1, keepdims=True),
+             jnp.sum(jnp.where(at_s >= at_t, steps, 0.0), axis=1, keepdims=True))
+    for j in range(8):
+        square, sine = half_turns(turn_2[j:j + 1, :] * reach[j // 4])
+        e = jnp.exp(-decay_2[j:j + 1, :] * reach[j // 4])
+        p_row[1, :, j * 128:(j + 1) * 128] = (e * (1.0 - 2.0 * square)).astype(BF16)
+        p_row[1, :, states + j * 128:states + (j + 1) * 128] = (e * sine).astype(BF16)
+    crossing(conv_b, kept_b, 1)
 
     repeat(1, n_sp, lambda r: interval_copy(r).wait_recv())
 
     def both_of(full, d):
         return jnp.concatenate([full[d * 4:d * 4 + 4], full[d * 4:d * 4 + 4]], axis=0)
 
-    def init_of(d):
+    def init_of(s, d):
+        ref = init_ref.at[s]
         parts = [
-            jnp.concatenate([init_ref[pl.ds(d * 16 + part * 8, 4, stride=2), :],
-                             init_ref[pl.ds(d * 16 + part * 8 + 1, 4, stride=2), :]], axis=1)
+            jnp.concatenate([ref[pl.ds(d * 16 + part * 8, 4, stride=2), :],
+                             ref[pl.ds(d * 16 + part * 8 + 1, 4, stride=2), :]], axis=1)
             for part in range(2)
         ]
         return jnp.concatenate(parts, axis=0)
 
-    decays = [both_of(decay, d) for d in range(2)]
-    turns = [both_of(turn, d) for d in range(2)]
+    decays = [[both_of(full, d) for d in range(2)] for full in (decay, decay_2)]
+    turns = [[both_of(full, d) for d in range(2)] for full in (turn, turn_2)]
 
     def weight(damping, turning, span):
         square, sine = half_turns(turning * span)
@@ -432,9 +517,10 @@
         r = n_sp - i
         mine = sp - r >= 0
         span = jnp.where(mine, span_ref[r], jnp.broadcast_to(total, (1, 128)))
-        w = weight(jnp.where(mine, decays[0], decays[1]), jnp.where(mine, turns[0], turns[1]), span)
-        wa_ref[r] = w[0]
-        wb_ref[r] = w[1]
+        for s in range(2):
+            w = weight(jnp.where(mine, *decays[s]), jnp.where(mine, *turns[s]), span)
+            wa_ref[s, r] = w[0]
+            wb_ref[s, r] = w[1]
         return total + elapsed(r)
 
     fold(1, n_sp, behind, none)
@@ -444,62 +530,61 @@
         return acc + elapsed(r) * jnp.where(sp - r >= 0, 0.0, 1.0)
 
     outside = fold(1, n_sp, beyond, none)
-    h0 = apply(weight(decays[0], turns[0], inside), init_of(0))
-    h1 = apply(weight(decays[1], turns[1], outside), init_of(1))
-
-    first.wait_recv()
-    c_out[...] = (acc_ref[...] + p1_in[...].astype(F32)).astype(BF16)
-    cross = remote(c_out, c_in, ps_sem.at[2], pr_sem.at[2], {"tp": oth})
-    cross.start()
-    mine = partial(tp)
-    second.wait_recv()
-    acc_ref[...] = mine + p2_in[...].astype(F32)
-
-    repeat(1, n_sp, lambda r: edge_copy(r).wait_recv())
-
-    def combine(r, carry):
-        h0, h1 = carry
-        moved = apply((wa_ref[r], wb_ref[r]), e_all[r])
-        mine = sp - r >= 0
-        return h0 + jnp.where(mine, moved, 0.0), h1 + jnp.where(mine, 0.0, moved)
-
-    entering = fold(1, n_sp, combine, (h0, h1))
-    for d in range(2):
-        for g in range(channels // group):
-            q = g // 2
-            hr, hi = entering[d][q:q + 1, :], entering[d][4 + q:5 + q, :]
-            cr_, ci_ = cc_ref[0, d, g], cc_ref[1, d, g]
-            at, lanes = pl.ds(g * group, group), pl.ds(d * half + q * 128, 128)
-            rc_ref[0, at, lanes] = (cr_ * hr - ci_ * hi).astype(BF16)
-            rc_ref[1, at, lanes] = (-(cr_ * hi + ci_ * hr)).astype(BF16)
-    for part in range(2):
-        response = response + dot_t(p_row[part], rc_ref[part])
-    inner = 0.7978845608028654 * (response + 0.044715 * (response * response * response))
-    state_out = (0.5 * response * (1.0 + jnp.tanh(inner))).astype(BF16)
+    from_start = [
+        tuple(apply(weight(decays[s][d], turns[s][d], (inside, outside)[d]), init_of(s, d))
+              for d in range(2))
+        for s in range(2)
+    ]
+
+    rest_copy.wait_recv()
+    edges(lambda copy: copy.wait_recv())
+    for s in range(2):
+        def combine(r, carry):
+            h0, h1 = carry
+            moved = apply((wa_ref[s, r], wb_ref[s, r]), e_all[s, r])
+            mine = sp - r >= 0
+            return h0 + jnp.where(mine, moved, 0.0), h1 + jnp.where(mine, 0.0, moved)
+
+        entering = fold(1, n_sp, combine, from_start[s])
+        for d in range(2):
+            for q in range(channels // group // 2):
+                hr, hi = entering[d][q:q + 1, :], entering[d][4 + q:5 + q, :]
+                cr, ci = (cq_ref[s, part, d, q].astype(F32) for part in range(2))
+                for part, value in ((0, cr * hr - ci * hi), (1, -(cr * hi + ci * hr))):
+                    for side in range(2):
+                        at = pl.ds((2 * q + side) * group, group)
+                        lanes = pl.ds(part * states + d * half + q * 128, 128)
+                        rc_ref[s, at, lanes] = jnp.where(
+                            left if side == 0 else ~left, value, 0.0).astype(BF16)
+    gated = []
+    for s in range(2):
+        full = response if s == 0 else rp_in[...].astype(F32)
+        full = full + dot_t(p_row[s], rc_ref[s])
+        inner = 0.7978845608028654 * (full + 0.044715 * (full * full * full))
+        gated.append((0.5 * full * (1.0 + jnp.tanh(inner))).astype(BF16))
+    state_out = jnp.concatenate(gated, axis=1)
     so_ref[...] = state_out
-    state_copies = [
-        remote(so_ref, so_all.at[tp], ss_sem.at[i], sr_sem.at[i], {"tp": peer})
-        for i, peer in enumerate(peers)
-    ]
-    for copy in state_copies:
-        copy.start()
-    total = acc_ref[...] + dot(state_out, ps_v[tp])
-    for copy in weight_copies:
+    state_copy = remote(so_ref, so_in, ss_sem.at[0], sr_sem.at[0], {"tp": sib})
+    state_copy.start()
+    for copy in weight_forward:
         copy.wait_recv()
-    cross.wait_recv()
-    total = total + c_in[...].astype(F32)
-    for i in (2, 0, 1):
-        state_copies[i].wait_recv()
-        total = total + dot(so_all[peers[i]], ps_v[peers[i]])
-    out_ref[...] = total.astype(BF16)
+    total = dot(state_out, ps_v[:2 * channels])
+    for copies in (conv_a, conv_b):
+        for copy in copies[1:]:
+            copy.wait_recv()
+    base = acc_ref[...] + p2_in[...].astype(F32) + c_in[...].astype(F32)
+    total = total + jnp.concatenate(
+        [base[inner_rows:inner_rows + edge], base[:inner_rows], base[inner_rows + edge:]], axis=0)
+    state_copy.wait_recv()
+    out_ref[...] = (total + dot(so_in[...], ps_v[2 * channels:])).astype(BF16)
 
     pl.when(not_last)(halo_up.wait_send)
     pl.when(not_first)(halo_down.wait_send)
-    for copy in (to_sib + to_oth + forward + gain_copies + weight_copies + state_copies
-                 + [first, second, cross]):
+    for copy in (to_sib + forward + gain_copies + weight_copies + weight_forward + other_copies
+                 + conv_a + conv_b + [rest_copy, state_copy]):
         copy.wait_send()
     repeat(1, n_sp, lambda r: interval_copy(r).wait_send())
-    repeat(1, n_sp, lambda r: edge_copy(r).wait_send())
+    edges(lambda copy: copy.wait_send())
 
 
 def per_device(
@@ -526,13 +611,14 @@
             pltpu.VMEM((1, width), F32),
             pltpu.VMEM(conv_taps.shape, F32),
             pltpu.VMEM((1, channels), F32),
-            pltpu.VMEM((dirs * groups, per), F32),
-            pltpu.VMEM((dirs * groups, per), F32),
-            pltpu.VMEM((dirs * 2 * groups, per), F32),
+            pltpu.VMEM((2, dirs * groups, per), F32),
+            pltpu.VMEM((2, dirs * groups, per), F32),
+            pltpu.VMEM((2, dirs * 2 * groups, per), F32),
             pltpu.SMEM((1, rows), F32),
+            pltpu.VMEM((1, rows), F32),
             pltpu.VMEM((width * n_tp, 4 * channels), BF16),
             pltpu.VMEM((channels, width * n_tp), BF16),
-            pltpu.VMEM((n_tp, channels, width), BF16),
+            pltpu.VMEM((n_tp * channels, width), BF16),
             pltpu.VMEM((2, dirs * groups * group, per), F32),
             pltpu.VMEM((2, dirs * groups * group, per), F32),
             pltpu.VMEM((n_tp, CHUNKS, rows, cw), BF16),
@@ -541,26 +627,31 @@
             packed, packed, packed, packed, packed, packed, packed, packed, packed, packed,
             pltpu.VMEM((2, rows, states), F32),
             pltpu.VMEM((2, rows, states), F32),
-            pltpu.VMEM((2, rows, states), BF16),
+            pltpu.VMEM((2, rows, 2 * states), BF16),
             pltpu.VMEM((2, channels, states), BF16),
             pltpu.VMEM((2, channels, states), BF16),
-            pltpu.VMEM((2, channels, states), BF16),
-            pltpu.VMEM((2, dirs, groups, group, 2 * per), F32),
+            pltpu.VMEM((2, channels, 2 * states), BF16),
+            pltpu.VMEM((2, 2, dirs, groups // 2, group, 2 * per), BF16),
             pltpu.VMEM((rows, channels), BF16),
             pltpu.VMEM((2, 16, channels), BF16),
             pltpu.VMEM((2, 8, 128), F32),
-            pltpu.VMEM((n_sp, 8, 128), F32),
+            pltpu.VMEM((2, n_sp, 8, 128), F32),
             pltpu.VMEM((n_sp, 1, 128), F32),
-            pltpu.VMEM((n_sp, 8, 128), F32),
-            pltpu.VMEM((n_sp, 8, 128), F32),
+            pltpu.VMEM((2, n_sp, 8, 128), F32),
+            pltpu.VMEM((2, n_sp, 8, 128), F32),
         ] + [pltpu.VMEM((rows, width), BF16)] * 6 + [
             pltpu.VMEM((rows, width), F32),
+            pltpu.VMEM((rows, 2 * channels), BF16),
+            pltpu.VMEM((rows, 2 * channels), BF16),
             pltpu.VMEM((rows, channels), BF16),
-            pltpu.VMEM((n_tp, rows, channels), BF16),
-            dma(18),
+            pltpu.VMEM((rows, channels), BF16),
+            pltpu.VMEM((rows - 32, width), F32),
+        ] + [
+            dma(19),
             dma(CHUNKS), dma(CHUNKS), dma(CHUNKS), dma(CHUNKS), dma(CHUNKS), dma(CHUNKS),
-            dma(n_tp), dma(n_tp), dma(n_sp), dma(n_sp), dma(2), dma(2), dma(n_sp), dma(n_sp),
-            dma(3), dma(3), dma(3), dma(3), dma(3), dma(3),
+            dma(n_tp), dma(n_tp), dma(n_sp), dma(n_sp), dma(2), dma(2),
+            pltpu.SemaphoreType.DMA((2, n_sp)), pltpu.SemaphoreType.DMA((2, n_sp)),
+            dma(6), dma(6), dma(5), dma(5), dma(1), dma(1), dma(5), dma(5),
             pltpu.SemaphoreType.REGULAR((max(2, (n_sp - 1).bit_length()),)),
         ],
         compiler_params=pltpu.CompilerParams(

time: 22.9 us -> 20.3 us (0.89)
  Pallas kernels: 22 us -> 19.5 us
    pallas_call x1, Pallas kernels: 22 us -> 19.5 us  [per_device(): pl.pallas_call(functools.partial(kernel, n_sp, n_tp), out_shape=jax.Shape...]
where the time goes in v2:
time: 20.3 us; the launch traced here: 20.2 us
  Pallas kernels  19.5 us (96%)
  local copies, waits for them, and re-layouts  0.66 us (3%)
    pallas_call x1, Pallas kernels, per_device(): pl.pallas_call(functools.partial(kernel, n_sp, n_tp), out_shape=jax.Shape...  19.5 us
    unnamed x1, local copies, waits for them, and re-layouts  0.66 us

profile of v2, /device:TPU:0, one launch (start us, length us, event | category | flops | bytes accessed | tf_op | source)
XLA Modules:
  0.0 20.2 jit_solution(14073722005084818762)
XLA Ops:
  0.0 19.5 %shard_map.172 = bf16[128,512]{1,0:T(8,128)(2,1)S(1)} custom-call(bf16[128,512]{1,0:T(8,128)(2,1)} %x_hbm.1, f32[1,512]{1,0:T(1,128)} %bitcast.21, bf16[2048,128]{1,0:T(8,128)(2,1)} %wv.1, bf16[2048,128]{1,0:T(8,128)(2,1)} %wm.1, bf16[2048,128]{1,0:T(8,128)(2,1)} %wg.1, bf16[2048,128]{1,0:T(8,128)(2,1)} %ws.1, f32[3,128]{1,0:T(4,128)} %taps_hbm.1, ...), custom_call_target="tpu_custom_call" | custom-call | tf_op jit(solution)/shard_map/pallas_call | solution.py:604
  19.5 0.7 %copy.20 = bf16[128,512]{1,0:T(8,128)(2,1)} copy(bf16[128,512]{1,0:T(8,128)(2,1)S(1)} %shard_map.172) | data formatting | bytes 262144

commit v3 on v2

--- a/solution.py
+++ b/solution.py
@@ -71,14 +71,13 @@
     x_hbm, gain_hbm, wv, wm, wg, ws, taps_hbm, skip_hbm, decay_hbm, turn_hbm,
     inr, ini, rdr, rdi, init_hbm, iv_hbm, pc, ps,
     out_ref,
-    x_ref, gain_ref, taps_ref, skip_ref, decay_ref, turn_ref, init_ref, iv_s, iv_v,
+    x_ref, gain_ref, taps_ref, skip_ref, par_ref, iv_s, iv_v,
     w_all, pc_v, ps_v, in_v, rd_v, x_full, gains, el_all, fr_ref, fi_ref, gr_ref, gi_ref,
     dr_ref, di_ref, hr_ref, hi_ref, kr_ref, ki_ref, k_row, d_row, p_row,
     bt_ref, rt_ref, rc_ref, cq_ref, src_ref, halo_ref, e_out, e_all,
-    span_ref, wa_ref, wb_ref, p1_out, p1_in, p2_out, p2_in, c_out, c_in, acc_ref, so_ref, so_in,
+    span_ref, wa_ref, wb_ref, po_ref, p1_in, pi_ref, acc_ref, so_ref, so_in,
     rp_out, rp_in, kept_ref,
-    load_sem, as_sem, ar_sem, bs_sem, br_sem, fs_sem, fwr_sem, gs_sem, grv_sem,
-    is_sem, ir_sem, hs_sem, hr_sem, es_sem, er_sem, ps_sem, pr_sem, ws_sem, wr_sem, ss_sem, sr_sem, os_sem, or_sem, greet_sem,
+    load_sem, fwr_sem, br_sem, one_sem, hs_sem, hr_sem, p1r_sem, greet_sem, pair_sem,
 ):
     tp, sp = lax.axis_index("tp"), lax.axis_index("sp")
     rows, width = x_hbm.shape
@@ -89,16 +88,28 @@
     diag = (1 - y) * 2 + 1 - core
     cw = width // CHUNKS
 
+    names = ("bs", "as", "ar", "fs", "gs", "gr", "is", "ir", "es", "er", "ps", "pr", "ws", "wr",
+             "vs", "vr", "os", "or", "cs", "cr", "rs", "rr", "ss", "sr")
+    one = {name: one_sem.at[i] for i, name in enumerate(names)}
     loads = {}
 
-    def load(name, src, dst):
-        copy = pltpu.make_async_copy(src, dst, load_sem.at[len(loads)])
-        copy.start()
-        loads[name] = copy
+    def load(name, whole, *pairs):
+        sem = load_sem.at[len(loads)]
+        loads[name] = whole, sem
+        for src, dst in pairs:
+            pltpu.make_async_copy(src, dst, sem).start()
+
+    def remote(src, dst, send, recv, where):
+        return pltpu.make_async_remote_copy(
+            src_ref=src, dst_ref=dst, send_sem=send, recv_sem=recv,
+            device_id=where, device_id_type=MESH)
+
+    def drain(ref, sem):
+        remote(ref, ref, sem, sem, {"tp": sib}).wait_recv()
 
     def loaded(*names):
         for name in names:
-            loads[name].wait()
+            drain(*loads[name])
 
     def near(step, act):
         for s in (-step, step):
@@ -118,52 +129,49 @@
 
     rounds = greet_sem.shape[0]
     barrier = pltpu.get_barrier_semaphore()
-    for j in range(1, n_tp):
-        pl.semaphore_signal(barrier, inc=1, device_id={"tp": (tp + j) % n_tp}, device_id_type=MESH)
+    for peer in (sib, oth):
+        pl.semaphore_signal(barrier, inc=1, device_id={"tp": peer}, device_id_type=MESH)
     near(1, lambda where: pl.semaphore_signal(
         barrier, inc=1, device_id={"sp": where}, device_id_type=MESH))
-    load("x", x_hbm, x_ref)
-    load("iv", iv_hbm, iv_s)
-    load("ivv", iv_hbm, iv_v)
-    load("decay", decay_hbm, decay_ref.at[0])
-    load("turn", turn_hbm, turn_ref.at[0])
-    load("init", init_hbm, init_ref.at[0])
-    load("gain", gain_hbm, gain_ref)
-    load("inr", inr, in_v.at[0])
-    load("ini", ini, in_v.at[1])
-    load("rdr", rdr, rd_v.at[0])
-    load("rdi", rdi, rd_v.at[1])
-    for j, w in enumerate((wv, wm, wg, ws)):
-        load("w%d" % j, w, w_all.at[:, pl.ds(j * channels, channels)])
-    load("taps", taps_hbm, taps_ref)
-    load("skip", skip_hbm, skip_ref)
-    load("pc", pc, pc_v)
-    load("ps", ps.at[:, pl.ds(pl.multiple_of(tp * width, width), width)], ps_v.at[pl.ds(0, channels)])
-    pl.semaphore_wait(barrier, n_tp - 1 + near_count(1))
+    load("x", x_ref, (x_hbm, x_ref))
+    iv_load = pltpu.make_async_copy(iv_hbm, iv_s, load_sem.at[len(loads)])
+    iv_load.start()
+    loads["iv"] = None
+    dirs_groups = decay_hbm.shape[0]
+    par_parts = (pl.ds(0, dirs_groups), pl.ds(dirs_groups, dirs_groups),
+                 pl.ds(2 * dirs_groups, 2 * dirs_groups))
+    par_hbm = (decay_hbm, turn_hbm, init_hbm)
+    load("par", par_ref.at[0], *((src, par_ref.at[0, at]) for src, at in zip(par_hbm, par_parts)))
+    load("ivv", iv_v, (iv_hbm, iv_v))
+    load("gain", gain_ref, (gain_hbm, gain_ref))
+    load("in", in_v, (inr, in_v.at[0]), (ini, in_v.at[1]))
+    load("rd", rd_v, (rdr, rd_v.at[0]), (rdi, rd_v.at[1]))
+    load("w", w_all, *((w, w_all.at[:, pl.ds(j * channels, channels)])
+                       for j, w in enumerate((wv, wm, wg, ws))))
+    load("taps", taps_ref, (taps_hbm, taps_ref))
+    load("skip", skip_ref, (skip_hbm, skip_ref))
+    load("pc", pc_v, (pc, pc_v))
+    own = ps.at[:, pl.ds(pl.multiple_of(tp * width, width), width)]
+    load("ps", ps_v.at[pl.ds(0, channels)], (own, ps_v.at[pl.ds(0, channels)]))
+    pl.semaphore_wait(barrier, 2 + near_count(1))
     loaded("x")
-
-    def remote(src, dst, send, recv, where):
-        return pltpu.make_async_remote_copy(
-            src_ref=src, dst_ref=dst, send_sem=send, recv_sem=recv,
-            device_id=where, device_id_type=MESH)
 
     to_sib, to_oth, forward = [], [], []
     for c in range(CHUNKS):
         piece = x_ref.at[:, pl.ds(c * cw, cw)]
-        to_oth.append(remote(piece, x_full.at[tp, c], bs_sem.at[c], br_sem.at[c], {"tp": oth}))
-        to_sib.append(remote(piece, x_full.at[tp, c], as_sem.at[c], ar_sem.at[c], {"tp": sib}))
-        forward.append(remote(x_full.at[oth, c], x_full.at[oth, c], fs_sem.at[c], fwr_sem.at[c],
+        to_oth.append(remote(piece, x_full.at[tp, c], one["bs"], br_sem.at[c], {"tp": oth}))
+        to_sib.append(remote(piece, x_full.at[tp, c], one["as"], one["ar"], {"tp": sib}))
+        forward.append(remote(x_full.at[oth, c], x_full.at[oth, c], one["fs"], fwr_sem.at[c],
                               {"tp": sib}))
     for c in range(CHUNKS):
         to_oth[c].start()
     for c in range(CHUNKS):
         to_sib[c].start()
     gain_copies = [
-        remote(gain_hbm, gains.at[tp], gs_sem.at[j], grv_sem.at[j], {"tp": (tp + j) % n_tp})
+        remote(gain_hbm, gains.at[j], one["gs"], one["gr"], {"tp": (tp + j) % n_tp})
         for j in range(1, n_tp)
     ]
-    for copy in gain_copies:
-        copy.start()
+    pl.semaphore_signal(pair_sem, inc=1, device_id={"tp": sib}, device_id_type=MESH)
     greet(0)
     part_rows = channels // 2
     my_part = pl.multiple_of((sp % 2) * part_rows, part_rows)
@@ -176,24 +184,21 @@
         return ps_v.at[pl.ds(pos * channels + my_part, part_rows)]
 
     weight_copies = [
-        remote(ps.at[:, columns(sib)], ps_v.at[pl.ds(2 * channels, channels)],
-               ws_sem.at[0], wr_sem.at[0], {"tp": sib}),
-        remote(ps.at[pl.ds(my_part, part_rows), columns(oth)], slot(1), ws_sem.at[1], wr_sem.at[1],
-               {"tp": oth}),
-        remote(ps.at[pl.ds(my_part, part_rows), columns(diag)], slot(3), ws_sem.at[2], wr_sem.at[2],
-               {"tp": diag}),
+        remote(src, dst, one["ws"], one["wr"], {"tp": peer})
+        for src, dst, peer in (
+            (ps.at[pl.ds(my_part, part_rows), columns(oth)], slot(1), oth),
+            (ps.at[pl.ds(my_part, part_rows), columns(diag)], slot(3), diag),
+            (ps.at[:, columns(sib)], ps_v.at[pl.ds(2 * channels, channels)], sib),
+        )
     ]
     weight_forward = [
-        remote(slot(pos), slot(pos), ws_sem.at[3 + i], wr_sem.at[3 + i], {"sp": twin})
-        for i, pos in enumerate((1, 3))
+        remote(slot(pos), slot(pos), one["vs"], one["vr"], {"sp": twin}) for pos in (1, 3)
     ]
     other_copies = [
-        remote(src, dst, os_sem.at[i], or_sem.at[i], {"tp": oth})
-        for i, (src, dst) in enumerate((
-            (decay_hbm, decay_ref.at[1]), (turn_hbm, turn_ref.at[1]), (init_hbm, init_ref.at[1]),
-            (cq_ref.at[0], cq_ref.at[1])))
-    ]
-    rest_copy = remote(rp_out, rp_in, os_sem.at[4], or_sem.at[4], {"tp": oth})
+        remote(src, par_ref.at[1, at], one["os"], one["or"], {"tp": oth})
+        for src, at in zip(par_hbm, par_parts)
+    ] + [remote(cq_ref.at[0], cq_ref.at[1], one["cs"], one["cr"], {"tp": oth})]
+    rest_copy = remote(rp_out, rp_in, one["rs"], one["rr"], {"tp": oth})
 
     def pass_on(c):
         to_oth[c].wait_recv()
@@ -202,13 +207,14 @@
     sub = lax.broadcasted_iota(jnp.int32, (8, 128), 0)
     top = sub < 4
 
-    def pack(ref):
-        even = ref[pl.ds(0, 8, stride=2), :]
-        odd = ref[pl.ds(1, 8, stride=2), :]
+    def pack(s, first):
+        even = par_ref[s, pl.ds(first, 8, stride=2), :]
+        odd = par_ref[s, pl.ds(first + 1, 8, stride=2), :]
         return jnp.concatenate([even, odd], axis=1)
 
-    loaded("iv", "decay", "turn", "init")
-    decay, turn = pack(decay_ref.at[0]), pack(turn_ref.at[0])
+    iv_load.wait()
+    loaded("par")
+    decay, turn = pack(0, 0), pack(0, dirs_groups)
     den = decay * decay + turn * turn
     td, dd = turn / den, decay / den
 
@@ -231,6 +237,9 @@
     greeted(0)
     if rounds > 1:
         greet(1)
+    pl.semaphore_wait(pair_sem, 1)
+    for copy in gain_copies:
+        copy.start()
     lax.fori_loop(3 * rows // 4, rows, factors, 0, unroll=4)
 
     def put(ref, k, value):
@@ -251,8 +260,8 @@
         fr, fi = fr_ref[back, :], fi_ref[back, :]
         return ar, ai, fr * br - fi * bi, fr * bi + fi * br
 
-    one, zero = jnp.ones((8, 128), F32), jnp.zeros((8, 128), F32)
-    lax.fori_loop(0, rows, chain, (one, zero, one, zero), unroll=4)
+    unit, zero = jnp.ones((8, 128), F32), jnp.zeros((8, 128), F32)
+    lax.fori_loop(0, rows, chain, (unit, zero, unit, zero), unroll=4)
     if rounds > 1:
         greeted(1)
     for k in range(2, rounds):
@@ -266,12 +275,11 @@
             k_row[part, :, lanes] = k_ref[pl.ds(j, rows, stride=8), :]
             p_row[0, :, pl.ds(part * bt_ref.shape[2] + j * 128, 128)] = h_ref[pl.ds(j, rows, stride=8), :].astype(BF16)
     pass_on(1)
-    for copy in to_oth:
-        copy.wait_send()
+    drain(x_ref, one["bs"])
     for copy in weight_copies:
         copy.start()
 
-    loaded("inr", "ini", "rdr", "rdi")
+    loaded("in", "rd")
     states = bt_ref.shape[2]
     per = rd_v.shape[2]
     half = states // 2
@@ -298,9 +306,12 @@
     pass_on(2)
     for copy in other_copies:
         copy.start()
-    loaded("gain", "w0", "w1", "w2", "w3")
-    for copy in gain_copies:
-        copy.wait_recv()
+    loaded("gain", "w")
+    others = gains.at[pl.ds(1, n_tp - 1)]
+    drain(others, one["gr"])
+
+    def gain_of(owner):
+        return gains[(tp - owner + n_tp) % n_tp]
 
     def project(value, gain, first):
         wide = value.astype(F32)
@@ -316,11 +327,10 @@
 
     def whole(owner, projected, squares):
         value = jnp.concatenate([x_full[owner, c] for c in range(CHUNKS)], axis=1)
-        t, s = project(value, gains[owner], owner * width)
+        t, s = project(value, gain_of(owner), owner * width)
         return projected + t, squares + s
 
-    for c in range(CHUNKS):
-        to_sib[c].wait_recv()
+    drain(x_full.at[sib], one["ar"])
     projected, squares = whole(sib, projected, squares)
     pass_on(3)
     projected, squares = whole(oth, projected, squares)
@@ -328,12 +338,12 @@
         greeted(rounds - 1)
 
     def interval_copy(r):
-        return remote(iv_hbm, el_all.at[r], is_sem.at[r], ir_sem.at[r], {"sp": (sp + r) % n_sp})
+        return remote(iv_hbm, el_all.at[r], one["is"], one["ir"], {"sp": (sp + r) % n_sp})
 
     repeat(1, n_sp, lambda r: interval_copy(r).start())
     for c in range(CHUNKS):
         forward[c].wait_recv()
-        t, s = project(x_full[diag, c], gains[diag][:, c * cw:(c + 1) * cw], diag * width + c * cw)
+        t, s = project(x_full[diag, c], gain_of(diag)[:, c * cw:(c + 1) * cw], diag * width + c * cw)
         projected, squares = projected + t, squares + s
     projected = projected * lax.rsqrt(squares / (width * n_tp) + EPSILON)
     state_input = projected[:, 3 * channels:].astype(BF16)
@@ -358,8 +368,7 @@
 
 
     def edge_copy(r, s):
-        return remote(e_out.at[jnp.where(sp + r < n_sp, 0, 1)], e_all.at[s, r], es_sem.at[s, r],
-                      er_sem.at[s, r], {"sp": (sp + r) % n_sp, "tp": oth if s else tp})
+        return remote(e_out.at[jnp.where(sp + r < n_sp, 0, 1)], e_all.at[s, r], one["es"], one["er"], {"sp": (sp + r) % n_sp, "tp": oth if s else tp})
 
     def edges(act):
         def at(r):
@@ -395,13 +404,13 @@
     def products(branch, i):
         at = pieces[i]
         copies = [
-            remote(p1_out.at[at], p1_in.at[at], ps_sem.at[3 * i], pr_sem.at[3 * i], {"tp": sib}),
-            remote(p2_out.at[at], p2_in.at[at], ps_sem.at[3 * i + 1], pr_sem.at[3 * i + 1], {"tp": sib}),
-            remote(c_out.at[at], c_in.at[at], ps_sem.at[3 * i + 2], pr_sem.at[3 * i + 2], {"tp": oth}),
+            remote(po_ref.at[0, at], p1_in.at[at], one["ps"], p1r_sem.at[i], {"tp": sib}),
+            remote(po_ref.at[1, at], pi_ref.at[0, at], one["ps"], one["pr"], {"tp": sib}),
+            remote(po_ref.at[2, at], pi_ref.at[1, at], one["ps"], one["pr"], {"tp": oth}),
         ]
-        p1_out[at, :] = dot(branch, pc_v[:, columns(diag)]).astype(BF16)
+        po_ref[0, at, :] = dot(branch, pc_v[:, columns(diag)]).astype(BF16)
         copies[0].start()
-        p2_out[at, :] = dot(branch, pc_v[:, columns(sib)]).astype(BF16)
+        po_ref[1, at, :] = dot(branch, pc_v[:, columns(sib)]).astype(BF16)
         copies[1].start()
         kept = dot(branch, pc_v[:, columns(oth)])
         acc_ref[at, :] = dot(branch, pc_v[:, columns(tp)])
@@ -410,7 +419,7 @@
     def crossing(copies, kept, i):
         at = pieces[i]
         copies[0].wait_recv()
-        c_out[at, :] = (kept + p1_in[at, :].astype(F32)).astype(BF16)
+        po_ref[2, at, :] = (kept + p1_in[at, :].astype(F32)).astype(BF16)
         copies[2].start()
 
     conv_a, kept = products(conv_out, 0)
@@ -446,22 +455,11 @@
     rp_out[...] = response.astype(BF16)
     rest_copy.start()
     crossing(conv_a, kept_ref[...], 0)
-    for copy in weight_copies:
-        copy.wait_recv()
+    drain(ps_v.at[pl.ds(0, 2 * channels)], one["wr"])
     for copy in weight_forward:
         copy.start()
-    pl.when(not_first)(halo_up.wait_recv)
-    pl.when(not_last)(halo_down.wait_recv)
-    before = jnp.where(not_first, halo_ref[0].astype(F32)[15:16, :], 0.0) * taps_ref[0:1, :]
-    after = jnp.where(not_last, halo_ref[1].astype(F32)[0:1, :], 0.0) * taps_ref[2:3, :]
-    end_line = lax.broadcasted_iota(jnp.int32, (2 * edge, channels), 0)
-    end_filtered = end_filtered + jnp.where(
-        end_line == 0, before, jnp.where(end_line == 2 * edge - 1, after, 0.0))
-    conv_b, kept_b = products((end_gate * end_filtered).astype(BF16), 1)
-
-    for copy in other_copies:
-        copy.wait_recv()
-    decay_2, turn_2 = pack(decay_ref.at[1]), pack(turn_ref.at[1])
+    drain(par_ref.at[1], one["or"])
+    decay_2, turn_2 = pack(1, 0), pack(1, dirs_groups)
     at_t = lax.broadcasted_iota(jnp.int32, (rows, rows), 0)
     at_s = lax.broadcasted_iota(jnp.int32, (rows, rows), 1)
     loaded("ivv")
@@ -473,19 +471,27 @@
         e = jnp.exp(-decay_2[j:j + 1, :] * reach[j // 4])
         p_row[1, :, j * 128:(j + 1) * 128] = (e * (1.0 - 2.0 * square)).astype(BF16)
         p_row[1, :, states + j * 128:states + (j + 1) * 128] = (e * sine).astype(BF16)
-    crossing(conv_b, kept_b, 1)
-
-    repeat(1, n_sp, lambda r: interval_copy(r).wait_recv())
+    pl.when(not_first)(halo_up.wait_recv)
+    pl.when(not_last)(halo_down.wait_recv)
+    before = jnp.where(not_first, halo_ref[0].astype(F32)[15:16, :], 0.0) * taps_ref[0:1, :]
+    after = jnp.where(not_last, halo_ref[1].astype(F32)[0:1, :], 0.0) * taps_ref[2:3, :]
+    end_line = lax.broadcasted_iota(jnp.int32, (2 * edge, channels), 0)
+    end_filtered = end_filtered + jnp.where(
+        end_line == 0, before, jnp.where(end_line == 2 * edge - 1, after, 0.0))
+    conv_b, kept_b = products((end_gate * end_filtered).astype(BF16), 1)
+
+    far = pl.ds(1, n_sp - 1)
+    drain(el_all.at[far], one["ir"])
 
     def both_of(full, d):
         return jnp.concatenate([full[d * 4:d * 4 + 4], full[d * 4:d * 4 + 4]], axis=0)
 
     def init_of(s, d):
-        ref = init_ref.at[s]
+        starts = [2 * dirs_groups + d * 16 + part * 8 for part in range(2)]
         parts = [
-            jnp.concatenate([ref[pl.ds(d * 16 + part * 8, 4, stride=2), :],
-                             ref[pl.ds(d * 16 + part * 8 + 1, 4, stride=2), :]], axis=1)
-            for part in range(2)
+            jnp.concatenate([par_ref[s, pl.ds(at, 4, stride=2), :],
+                             par_ref[s, pl.ds(at + 1, 4, stride=2), :]], axis=1)
+            for at in starts
         ]
         return jnp.concatenate(parts, axis=0)
 
@@ -536,8 +542,11 @@
         for s in range(2)
     ]
 
+    crossing(conv_b, kept_b, 1)
+
     rest_copy.wait_recv()
-    edges(lambda copy: copy.wait_recv())
+    drain(cq_ref.at[1], one["cr"])
+    drain(e_all.at[:, far], one["er"])
     for s in range(2):
         def combine(r, carry):
             h0, h1 = carry
@@ -564,15 +573,12 @@
         gated.append((0.5 * full * (1.0 + jnp.tanh(inner))).astype(BF16))
     state_out = jnp.concatenate(gated, axis=1)
     so_ref[...] = state_out
-    state_copy = remote(so_ref, so_in, ss_sem.at[0], sr_sem.at[0], {"tp": sib})
+    state_copy = remote(so_ref, so_in, one["ss"], one["sr"], {"tp": sib})
     state_copy.start()
-    for copy in weight_forward:
-        copy.wait_recv()
+    drain(ps_v.at[pl.ds(0, channels)], one["vr"])
     total = dot(state_out, ps_v[:2 * channels])
-    for copies in (conv_a, conv_b):
-        for copy in copies[1:]:
-            copy.wait_recv()
-    base = acc_ref[...] + p2_in[...].astype(F32) + c_in[...].astype(F32)
+    drain(pi_ref, one["pr"])
+    base = acc_ref[...] + pi_ref[0].astype(F32) + pi_ref[1].astype(F32)
     total = total + jnp.concatenate(
         [base[inner_rows:inner_rows + edge], base[:inner_rows], base[inner_rows + edge:]], axis=0)
     state_copy.wait_recv()
@@ -580,11 +586,12 @@
 
     pl.when(not_last)(halo_up.wait_send)
     pl.when(not_first)(halo_down.wait_send)
-    for copy in (to_sib + forward + gain_copies + weight_copies + weight_forward + other_copies
-                 + conv_a + conv_b + [rest_copy, state_copy]):
-        copy.wait_send()
-    repeat(1, n_sp, lambda r: interval_copy(r).wait_send())
-    edges(lambda copy: copy.wait_send())
+    for ref, name in (
+            (x_ref, "as"), (x_ref, "fs"), (others, "gs"), (el_all.at[far], "is"),
+            (e_all.at[:, far], "es"), (po_ref, "ps"), (ps_v.at[pl.ds(0, 2 * channels)], "ws"),
+            (ps_v.at[pl.ds(0, channels)], "vs"), (par_ref.at[0], "os"), (cq_ref.at[0], "cs"),
+            (rp_out, "rs"), (so_ref, "ss")):
+        drain(ref, one[name])
 
 
 def per_device(
@@ -611,9 +618,7 @@
             pltpu.VMEM((1, width), F32),
             pltpu.VMEM(conv_taps.shape, F32),
             pltpu.VMEM((1, channels), F32),
-            pltpu.VMEM((2, dirs * groups, per), F32),
-            pltpu.VMEM((2, dirs * groups, per), F32),
-            pltpu.VMEM((2, dirs * 2 * groups, per), F32),
+            pltpu.VMEM((2, 4 * dirs * groups, per), F32),
             pltpu.SMEM((1, rows), F32),
             pltpu.VMEM((1, rows), F32),
             pltpu.VMEM((width * n_tp, 4 * channels), BF16),
@@ -639,20 +644,18 @@
             pltpu.VMEM((n_sp, 1, 128), F32),
             pltpu.VMEM((2, n_sp, 8, 128), F32),
             pltpu.VMEM((2, n_sp, 8, 128), F32),
-        ] + [pltpu.VMEM((rows, width), BF16)] * 6 + [
+            pltpu.VMEM((3, rows, width), BF16),
+            pltpu.VMEM((rows, width), BF16),
+            pltpu.VMEM((2, rows, width), BF16),
             pltpu.VMEM((rows, width), F32),
             pltpu.VMEM((rows, 2 * channels), BF16),
             pltpu.VMEM((rows, 2 * channels), BF16),
             pltpu.VMEM((rows, channels), BF16),
             pltpu.VMEM((rows, channels), BF16),
             pltpu.VMEM((rows - 32, width), F32),
-        ] + [
-            dma(19),
-            dma(CHUNKS), dma(CHUNKS), dma(CHUNKS), dma(CHUNKS), dma(CHUNKS), dma(CHUNKS),
-            dma(n_tp), dma(n_tp), dma(n_sp), dma(n_sp), dma(2), dma(2),
-            pltpu.SemaphoreType.DMA((2, n_sp)), pltpu.SemaphoreType.DMA((2, n_sp)),
-            dma(6), dma(6), dma(5), dma(5), dma(1), dma(1), dma(5), dma(5),
+            dma(12), dma(CHUNKS), dma(CHUNKS), dma(24), dma(2), dma(2), dma(2),
             pltpu.SemaphoreType.REGULAR((max(2, (n_sp - 1).bit_length()),)),
+            pltpu.SemaphoreType.REGULAR,
         ],
         compiler_params=pltpu.CompilerParams(
             collective_id=0, has_side_effects=True, vmem_limit_bytes=48 * 1024 * 1024),

time: 20.3 us -> 19.1 us (0.941)
  Pallas kernels: 19.5 us -> 18.3 us
    pallas_call x1, Pallas kernels: 19.5 us -> 18.3 us  [per_device(): pl.pallas_call(functools.partial(kernel, n_sp, n_tp), out_shape=jax.Shape...]
where the time goes in v3:
time: 19.1 us; the launch traced here: 19 us
  Pallas kernels  18.3 us (96%)
  local copies, waits for them, and re-layouts  0.66 us (3%)
    pallas_call x1, Pallas kernels, per_device(): pl.pallas_call(functools.partial(kernel, n_sp, n_tp), out_shape=jax.Shape...  18.3 us
    unnamed x1, local copies, waits for them, and re-layouts  0.66 us

profile of v3, /device:TPU:0, one launch (start us, length us, event | category | flops | bytes accessed | tf_op | source)
XLA Modules:
  0.0 19.0 jit_solution(1607583647382309912)
XLA Ops:
  0.0 18.3 %shard_map.172 = bf16[128,512]{1,0:T(8,128)(2,1)S(1)} custom-call(bf16[128,512]{1,0:T(8,128)(2,1)} %x_hbm.1, f32[1,512]{1,0:T(1,128)} %bitcast.21, bf16[2048,128]{1,0:T(8,128)(2,1)} %wv.1, bf16[2048,128]{1,0:T(8,128)(2,1)} %wm.1, bf16[2048,128]{1,0:T(8,128)(2,1)} %wg.1, bf16[2048,128]{1,0:T(8,128)(2,1)} %ws.1, f32[3,128]{1,0:T(4,128)} %taps_hbm.1, ...), custom_call_target="tpu_custom_call" | custom-call | tf_op jit(solution)/shard_map/pallas_call | solution.py:611
  18.3 0.7 %copy.20 = bf16[128,512]{1,0:T(8,128)(2,1)} copy(bf16[128,512]{1,0:T(8,128)(2,1)S(1)} %shard_map.172) | data formatting | bytes 262144

commit v4 on v3

--- a/solution.py
+++ b/solution.py
@@ -12,6 +12,7 @@
 F32 = jnp.float32
 BF16 = jnp.bfloat16
 CHUNKS = 4
+SHARE = 4
 
 
 def dot(a, b):
@@ -75,9 +76,9 @@
     w_all, pc_v, ps_v, in_v, rd_v, x_full, gains, el_all, fr_ref, fi_ref, gr_ref, gi_ref,
     dr_ref, di_ref, hr_ref, hi_ref, kr_ref, ki_ref, k_row, d_row, p_row,
     bt_ref, rt_ref, rc_ref, cq_ref, src_ref, halo_ref, e_out, e_all,
-    span_ref, wa_ref, wb_ref, po_ref, p1_in, pi_ref, acc_ref, so_ref, so_in,
-    rp_out, rp_in, kept_ref,
-    load_sem, fwr_sem, br_sem, one_sem, hs_sem, hr_sem, p1r_sem, greet_sem, pair_sem,
+    span_ref, wa_ref, wb_ref, po_ref, p1_in, pi_ref, pd_ref, acc_ref, so_ref, so_in,
+    rp_out, rp_in, xs_ref,
+    load_sem, fwr_sem, br_sem, gr_sem, one_sem, hs_sem, hr_sem, p1r_sem, greet_sem, pair_sem,
 ):
     tp, sp = lax.axis_index("tp"), lax.axis_index("sp")
     rows, width = x_hbm.shape
@@ -88,8 +89,8 @@
     diag = (1 - y) * 2 + 1 - core
     cw = width // CHUNKS
 
-    names = ("bs", "as", "ar", "fs", "gs", "gr", "is", "ir", "es", "er", "ps", "pr", "ws", "wr",
-             "vs", "vr", "os", "or", "cs", "cr", "rs", "rr", "ss", "sr")
+    names = ("bs", "as", "ar", "fs", "gs", "ds", "dr", "is", "ir", "es", "er", "ps", "pr", "ws", "wr",
+             "vs", "vr", "qr", "os", "or", "cs", "cr", "rs", "rr", "ss", "sr")
     one = {name: one_sem.at[i] for i, name in enumerate(names)}
     loads = {}
 
@@ -154,28 +155,44 @@
     own = ps.at[:, pl.ds(pl.multiple_of(tp * width, width), width)]
     load("ps", ps_v.at[pl.ds(0, channels)], (own, ps_v.at[pl.ds(0, channels)]))
     pl.semaphore_wait(barrier, 2 + near_count(1))
-    loaded("x")
-
-    to_sib, to_oth, forward = [], [], []
-    for c in range(CHUNKS):
-        piece = x_ref.at[:, pl.ds(c * cw, cw)]
-        to_oth.append(remote(piece, x_full.at[tp, c], one["bs"], br_sem.at[c], {"tp": oth}))
-        to_sib.append(remote(piece, x_full.at[tp, c], one["as"], one["ar"], {"tp": sib}))
-        forward.append(remote(x_full.at[oth, c], x_full.at[oth, c], one["fs"], fwr_sem.at[c],
-                              {"tp": sib}))
-    for c in range(CHUNKS):
-        to_oth[c].start()
-    for c in range(CHUNKS):
-        to_sib[c].start()
+    loaded("x", "gain")
+
+    last = CHUNKS - 1
+    half_rows = rows // 2
+    upper, lower = pl.ds(0, half_rows), pl.ds(half_rows, half_rows)
+
+    def block(ref, c, part=None):
+        return ref.at[:, pl.ds(c * cw, cw)] if part is None else ref.at[part, pl.ds(c * cw, cw)]
+
+    def landing(owner, c, part=None):
+        return x_full.at[owner, c] if part is None else x_full.at[owner, c, part]
+
+    spans = [(c, None) for c in range(last)] + [(last, upper), (last, lower)]
+    to_oth = [
+        remote(block(x_ref, *span), landing(tp, *span), one["bs"], br_sem.at[i], {"tp": oth})
+        for i, span in enumerate(spans)
+    ]
+    to_sib = remote(x_ref, xs_ref, one["as"], one["ar"], {"tp": sib})
+    forward = [
+        remote(landing(oth, *span), landing(oth, *span), one["fs"], fwr_sem.at[i], {"tp": sib})
+        for i, span in enumerate(spans[:-1])
+    ]
+    to_diag = remote(block(x_ref, *spans[-1]), landing(tp, *spans[-1]), one["ds"], one["dr"],
+                     {"tp": diag})
     gain_copies = [
-        remote(gain_hbm, gains.at[j], one["gs"], one["gr"], {"tp": (tp + j) % n_tp})
-        for j in range(1, n_tp)
+        remote(gain_ref, gains.at[j], one["gs"], gr_sem.at[j], {"tp": peer})
+        for j, peer in enumerate((oth, sib, diag))
     ]
+    gain_copies[0].start()
+    for copy in to_oth:
+        copy.start()
+    gain_copies[1].start()
+    to_sib.start()
     pl.semaphore_signal(pair_sem, inc=1, device_id={"tp": sib}, device_id_type=MESH)
     greet(0)
-    part_rows = channels // 2
-    my_part = pl.multiple_of((sp % 2) * part_rows, part_rows)
-    twin = sp + 1 - 2 * (sp % 2)
+    part_rows = channels // SHARE
+    my_part = pl.multiple_of((sp % SHARE) * part_rows, part_rows)
+    mates = [sp // SHARE * SHARE + (sp + k) % SHARE for k in range(1, SHARE)]
 
     def columns(owner):
         return pl.ds(pl.multiple_of(owner * width, width), width)
@@ -192,7 +209,8 @@
         )
     ]
     weight_forward = [
-        remote(slot(pos), slot(pos), one["vs"], one["vr"], {"sp": twin}) for pos in (1, 3)
+        remote(slot(pos), slot(pos), one["vs"], one["vr"], {"sp": mate})
+        for mate in mates for pos in (1, 3)
     ]
     other_copies = [
         remote(src, par_ref.at[1, at], one["os"], one["or"], {"tp": oth})
@@ -238,7 +256,9 @@
     if rounds > 1:
         greet(1)
     pl.semaphore_wait(pair_sem, 1)
-    for copy in gain_copies:
+    gain_copies[2].start()
+    to_diag.start()
+    for copy in other_copies[:-1]:
         copy.start()
     lax.fori_loop(3 * rows // 4, rows, factors, 0, unroll=4)
 
@@ -268,17 +288,9 @@
         greet(k)
         if k < rounds - 1:
             greeted(k)
-    pass_on(0)
-    for part, (k_ref, h_ref) in enumerate(((kr_ref, hr_ref), (ki_ref, hi_ref))):
-        for j in range(8):
-            lanes = slice(j * 128, (j + 1) * 128)
-            k_row[part, :, lanes] = k_ref[pl.ds(j, rows, stride=8), :]
-            p_row[0, :, pl.ds(part * bt_ref.shape[2] + j * 128, 128)] = h_ref[pl.ds(j, rows, stride=8), :].astype(BF16)
-    pass_on(1)
-    drain(x_ref, one["bs"])
+
     for copy in weight_copies:
         copy.start()
-
     loaded("in", "rd")
     states = bt_ref.shape[2]
     per = rd_v.shape[2]
@@ -303,92 +315,123 @@
                 cq_ref[0, part, d, q] = jnp.concatenate(pair, axis=1).astype(BF16)
     rc_ref[...] = jnp.zeros_like(rc_ref)
 
+    pass_on(0)
+    for part, (k_ref, h_ref) in enumerate(((kr_ref, hr_ref), (ki_ref, hi_ref))):
+        for j in range(8):
+            lanes = slice(j * 128, (j + 1) * 128)
+            k_row[part, :, lanes] = k_ref[pl.ds(j, rows, stride=8), :]
+            p_row[0, :, pl.ds(part * states + j * 128, 128)] = h_ref[pl.ds(j, rows, stride=8), :].astype(BF16)
+    pass_on(1)
+    other_copies[-1].start()
+    loaded("w")
+    state_lanes = slice(3 * channels, None)
+    conv_lanes = slice(0, 3 * channels)
+
+    def scaled(value, gain):
+        return (value.astype(F32) * gain).astype(BF16)
+
+    def power(value):
+        wide = value.astype(F32)
+        return jnp.sum(wide * wide, axis=1, keepdims=True)
+
+    def weight_rows(owner, first, count):
+        return pl.ds(pl.multiple_of(owner * width + first, cw), count)
+
+    def chunks_of(owner, count):
+        return jnp.concatenate([x_full[owner, c] for c in range(count)], axis=1)
+
+    def project(value, gain, owner, count):
+        return dot(scaled(value, gain), w_all[weight_rows(owner, 0, count), :]), power(value)
+
+    projected, squares = project(x_ref[...], gain_ref[...], tp, width)
+    drain(xs_ref, one["ar"])
+    gain_copies[1].wait_recv()
+    t, s = project(xs_ref[...], gains[1], sib, width)
+    projected, squares = projected + t, squares + s
     pass_on(2)
-    for copy in other_copies:
-        copy.start()
-    loaded("gain", "w")
-    others = gains.at[pl.ds(1, n_tp - 1)]
-    drain(others, one["gr"])
-
-    def gain_of(owner):
-        return gains[(tp - owner + n_tp) % n_tp]
-
-    def project(value, gain, first):
-        wide = value.astype(F32)
-        scaled = (wide * gain).astype(BF16)
-        k = value.shape[1]
-        term = dot(scaled, w_all[pl.ds(pl.multiple_of(first, k), k), :])
-        return term, jnp.sum(wide * wide, axis=1, keepdims=True)
-
-    projected = jnp.zeros((rows, 4 * channels), F32)
-    squares = jnp.zeros((rows, 1), F32)
-    t, s = project(x_ref[...], gain_ref[...], tp * width)
+    gain_copies[0].wait_recv()
+    t, s = project(chunks_of(oth, last), gains[0][:, :last * cw], oth, last * cw)
     projected, squares = projected + t, squares + s
-
-    def whole(owner, projected, squares):
-        value = jnp.concatenate([x_full[owner, c] for c in range(CHUNKS)], axis=1)
-        t, s = project(value, gain_of(owner), owner * width)
-        return projected + t, squares + s
-
-    drain(x_full.at[sib], one["ar"])
-    projected, squares = whole(sib, projected, squares)
     pass_on(3)
-    projected, squares = whole(oth, projected, squares)
     if rounds > 2:
         greeted(rounds - 1)
 
     def interval_copy(r):
-        return remote(iv_hbm, el_all.at[r], one["is"], one["ir"], {"sp": (sp + r) % n_sp})
-
+        return remote(iv_v, el_all.at[r], one["is"], one["ir"], {"sp": (sp + r) % n_sp})
+
+    loaded("ivv")
     repeat(1, n_sp, lambda r: interval_copy(r).start())
-    for c in range(CHUNKS):
+    gain_copies[2].wait_recv()
+    for c in range(last):
         forward[c].wait_recv()
-        t, s = project(x_full[diag, c], gain_of(diag)[:, c * cw:(c + 1) * cw], diag * width + c * cw)
-        projected, squares = projected + t, squares + s
-    projected = projected * lax.rsqrt(squares / (width * n_tp) + EPSILON)
-    state_input = projected[:, 3 * channels:].astype(BF16)
-    conv_value = projected[:, :channels].astype(BF16).astype(F32)
-    conv_mix = projected[:, channels:2 * channels].astype(BF16).astype(F32)
-    conv_gate = projected[:, 2 * channels:3 * channels].astype(BF16).astype(F32)
+    t, s = project(chunks_of(diag, last), gains[2][:, :last * cw], diag, last * cw)
+    projected, squares = projected + t, squares + s
+    to_oth[last + 1].wait_recv()
+    tails = []
+    for owner, at in ((oth, 0), (diag, 2)):
+        if owner is diag:
+            forward[last].wait_recv()
+            to_diag.wait_recv()
+        value = x_full[owner, last]
+        squares = squares + power(value)
+        tails.append((scaled(value, gains[at][:, last * cw:]), weight_rows(owner, last * cw, cw)))
+    inv_rms = lax.rsqrt(squares / (width * n_tp) + EPSILON)
+
+    def finish(lanes):
+        total = projected[:, lanes]
+        for value, at in tails:
+            total = total + dot(value, w_all[at, lanes])
+        return total * inv_rms
+
+    state_input = finish(state_lanes).astype(BF16)
+
+
+    def edge_copy(r, s):
+        return remote(e_out.at[jnp.where(sp + r < n_sp, 0, 1)], e_all.at[s, r], one["es"], one["er"],
+                      {"sp": (sp + r) % n_sp, "tp": oth if s else tp})
+
+    def send_edges(lo, hi):
+        def at(r, carry):
+            edge_copy(r, 0).start()
+            edge_copy(r, 1).start()
+            return carry
+        lax.fori_loop(lo, hi, at, 0)
+
+    def find_edges(d):
+        for i in range(2):
+            lanes = slice(d * half + i * 256, d * half + (i + 1) * 256)
+            dr = dot(state_input, bt_ref[0, :, lanes])
+            di = dot(state_input, bt_ref[1, :, lanes])
+            d_row[0, :, lanes] = dr
+            d_row[1, :, lanes] = di
+            kr, ki = k_row[0, :, lanes], k_row[1, :, lanes]
+            er = jnp.sum(kr * dr - ki * di, axis=0, keepdims=True)
+            ei = jnp.sum(kr * di + ki * dr, axis=0, keepdims=True)
+            for h in range(2):
+                q = i * 2 + h
+                e_out[d, q:q + 1, :] = er[:, h * 128:(h + 1) * 128]
+                e_out[d, 4 + q:5 + q, :] = ei[:, h * 128:(h + 1) * 128]
+
+    find_edges(1)
+    send_edges(n_sp - sp, n_sp)
+    convs = finish(conv_lanes)
+    conv_value = convs[:, :channels].astype(BF16).astype(F32)
+    conv_mix = convs[:, channels:2 * channels].astype(BF16).astype(F32)
+    conv_gate = convs[:, 2 * channels:].astype(BF16).astype(F32)
     src_ref[...] = (conv_mix * conv_value).astype(BF16)
-
-    for j in range(4):
-        lanes = slice(j * 256, (j + 1) * 256)
-        dr = dot(state_input, bt_ref[0, :, lanes])
-        di = dot(state_input, bt_ref[1, :, lanes])
-        d_row[0, :, lanes] = dr
-        d_row[1, :, lanes] = di
-        kr, ki = k_row[0, :, lanes], k_row[1, :, lanes]
-        er = jnp.sum(kr * dr - ki * di, axis=0, keepdims=True)
-        ei = jnp.sum(kr * di + ki * dr, axis=0, keepdims=True)
-        for h in range(2):
-            q = (j % 2) * 2 + h
-            e_out[j // 2, q:q + 1, :] = er[:, h * 128:(h + 1) * 128]
-            e_out[j // 2, 4 + q:5 + q, :] = ei[:, h * 128:(h + 1) * 128]
-
-
-    def edge_copy(r, s):
-        return remote(e_out.at[jnp.where(sp + r < n_sp, 0, 1)], e_all.at[s, r], one["es"], one["er"], {"sp": (sp + r) % n_sp, "tp": oth if s else tp})
-
-    def edges(act):
-        def at(r):
-            act(edge_copy(r, 0))
-            act(edge_copy(r, 1))
-        repeat(1, n_sp, at)
-
     halo_up = remote(src_ref.at[pl.ds(rows - 16, 16)], halo_ref.at[0], hs_sem.at[0], hr_sem.at[0],
                      {"sp": (sp + 1) % n_sp})
     halo_down = remote(src_ref.at[pl.ds(0, 16)], halo_ref.at[1], hs_sem.at[1], hr_sem.at[1],
                        {"sp": (sp + n_sp - 1) % n_sp})
-    edges(lambda copy: copy.start())
     not_first, not_last = sp > 0, sp < n_sp - 1
     pl.when(not_last)(halo_up.start)
     pl.when(not_first)(halo_down.start)
-
     loaded("taps", "skip", "pc", "ps")
     edge = 16
     inner_rows = rows - 2 * edge
-    pieces = (pl.ds(0, inner_rows), pl.ds(inner_rows, 2 * edge))
+    direct_rows = pd_ref.shape[0]
+    inner, outer = (0, inner_rows), (inner_rows, 2 * edge)
+    middle = (direct_rows, inner_rows - direct_rows)
     source = src_ref[...].astype(F32)
     line = lax.broadcasted_iota(jnp.int32, (rows, channels), 0)
     previous = jnp.where(line == 0, 0.0, pltpu.roll(source, 1, 0))
@@ -401,34 +444,47 @@
 
     end_gate, end_filtered = ends(conv_gate), ends(filtered)
 
-    def products(branch, i):
-        at = pieces[i]
-        copies = [
-            remote(po_ref.at[0, at], p1_in.at[at], one["ps"], p1r_sem.at[i], {"tp": sib}),
-            remote(po_ref.at[1, at], pi_ref.at[0, at], one["ps"], one["pr"], {"tp": sib}),
-            remote(po_ref.at[2, at], pi_ref.at[1, at], one["ps"], one["pr"], {"tp": oth}),
-        ]
+    def offer(branch, i, span):
+        at = pl.ds(*span)
         po_ref[0, at, :] = dot(branch, pc_v[:, columns(diag)]).astype(BF16)
-        copies[0].start()
+        copy = remote(po_ref.at[0, at], p1_in.at[at], one["ps"], p1r_sem.at[i], {"tp": sib})
+        copy.start()
+        return copy
+
+    def crossing(branch, span):
+        at = pl.ds(*span)
+        kept = dot(branch, pc_v[:, columns(oth)])
+        po_ref[2, at, :] = (kept + p1_in[at, :].astype(F32)).astype(BF16)
+        copy = remote(po_ref.at[2, at], pi_ref.at[1, at], one["ps"], one["pr"], {"tp": oth})
+        copy.start()
+
+    def rest_of(branch, span):
+        at = pl.ds(*span)
         po_ref[1, at, :] = dot(branch, pc_v[:, columns(sib)]).astype(BF16)
-        copies[1].start()
-        kept = dot(branch, pc_v[:, columns(oth)])
+        copy = remote(po_ref.at[1, at], pi_ref.at[0, at], one["ps"], one["pr"], {"tp": sib})
+        copy.start()
         acc_ref[at, :] = dot(branch, pc_v[:, columns(tp)])
-        return copies, kept
-
-    def crossing(copies, kept, i):
-        at = pieces[i]
-        copies[0].wait_recv()
-        po_ref[2, at, :] = (kept + p1_in[at, :].astype(F32)).astype(BF16)
-        copies[2].start()
-
-    conv_a, kept = products(conv_out, 0)
-    kept_ref[...] = kept
+
+    direct = pl.ds(0, direct_rows)
+    direct_copies = [
+        remote(po_ref.at[2, direct], pi_ref.at[1, direct], one["ps"], one["pr"], {"tp": oth}),
+        remote(po_ref.at[0, direct], pd_ref, one["ps"], one["qr"], {"tp": diag}),
+    ]
+    for copy, at, owner in zip(direct_copies, (2, 0), (oth, diag)):
+        po_ref[at, direct, :] = dot(conv_out[:direct_rows], pc_v[:, columns(owner)]).astype(BF16)
+        copy.start()
+    offered = offer(conv_out[direct_rows:], 0, middle)
+
+    find_edges(0)
 
     for part, ref in ((0, dr_ref), (1, di_ref)):
         for j in range(8):
             ref[pl.ds(j, rows, stride=8), :] = d_row[part, :, j * 128:(j + 1) * 128]
 
+    send_edges(1, n_sp - sp)
+    drain(ps_v.at[pl.ds(0, channels + 2 * part_rows)], one["wr"])
+    for copy in weight_forward:
+        copy.start()
 
     def local(k, carry):
         hr, hi = carry
@@ -454,23 +510,8 @@
 
     rp_out[...] = response.astype(BF16)
     rest_copy.start()
-    crossing(conv_a, kept_ref[...], 0)
-    drain(ps_v.at[pl.ds(0, 2 * channels)], one["wr"])
-    for copy in weight_forward:
-        copy.start()
-    drain(par_ref.at[1], one["or"])
-    decay_2, turn_2 = pack(1, 0), pack(1, dirs_groups)
-    at_t = lax.broadcasted_iota(jnp.int32, (rows, rows), 0)
-    at_s = lax.broadcasted_iota(jnp.int32, (rows, rows), 1)
-    loaded("ivv")
-    steps = iv_v[...]
-    reach = (jnp.sum(jnp.where(at_s <= at_t, steps, 0.0), axis=1, keepdims=True),
-             jnp.sum(jnp.where(at_s >= at_t, steps, 0.0), axis=1, keepdims=True))
-    for j in range(8):
-        square, sine = half_turns(turn_2[j:j + 1, :] * reach[j // 4])
-        e = jnp.exp(-decay_2[j:j + 1, :] * reach[j // 4])
-        p_row[1, :, j * 128:(j + 1) * 128] = (e * (1.0 - 2.0 * square)).astype(BF16)
-        p_row[1, :, states + j * 128:states + (j + 1) * 128] = (e * sine).astype(BF16)
+    offered.wait_recv()
+    crossing(conv_out[direct_rows:], middle)
     pl.when(not_first)(halo_up.wait_recv)
     pl.when(not_last)(halo_down.wait_recv)
     before = jnp.where(not_first, halo_ref[0].astype(F32)[15:16, :], 0.0) * taps_ref[0:1, :]
@@ -478,8 +519,29 @@
     end_line = lax.broadcasted_iota(jnp.int32, (2 * edge, channels), 0)
     end_filtered = end_filtered + jnp.where(
         end_line == 0, before, jnp.where(end_line == 2 * edge - 1, after, 0.0))
-    conv_b, kept_b = products((end_gate * end_filtered).astype(BF16), 1)
-
+    conv_ends = (end_gate * end_filtered).astype(BF16)
+    offered_ends = offer(conv_ends, 1, outer)
+    rest_of(conv_out, inner)
+
+    drain(par_ref.at[1], one["or"])
+    decay_2, turn_2 = pack(1, 0), pack(1, dirs_groups)
+    at_t = lax.broadcasted_iota(jnp.int32, (rows, rows), 0)
+    at_s = lax.broadcasted_iota(jnp.int32, (rows, rows), 1)
+    steps = iv_v[...]
+    reach = (jnp.sum(jnp.where(at_s <= at_t, steps, 0.0), axis=1, keepdims=True),
+             jnp.sum(jnp.where(at_s >= at_t, steps, 0.0), axis=1, keepdims=True))
+    def reach_factors(j):
+        square, sine = half_turns(turn_2[j:j + 1, :] * reach[j // 4])
+        e = jnp.exp(-decay_2[j:j + 1, :] * reach[j // 4])
+        p_row[1, :, j * 128:(j + 1) * 128] = (e * (1.0 - 2.0 * square)).astype(BF16)
+        p_row[1, :, states + j * 128:states + (j + 1) * 128] = (e * sine).astype(BF16)
+    for j in range(4):
+        reach_factors(j)
+    offered_ends.wait_recv()
+    crossing(conv_ends, outer)
+    for j in range(4, 8):
+        reach_factors(j)
+    rest_of(conv_ends, outer)
     far = pl.ds(1, n_sp - 1)
     drain(el_all.at[far], one["ir"])
 
@@ -541,8 +603,6 @@
               for d in range(2))
         for s in range(2)
     ]
-
-    crossing(conv_b, kept_b, 1)
 
     rest_copy.wait_recv()
     drain(cq_ref.at[1], one["cr"])
@@ -575,21 +635,24 @@
     so_ref[...] = state_out
     state_copy = remote(so_ref, so_in, one["ss"], one["sr"], {"tp": sib})
     state_copy.start()
-    drain(ps_v.at[pl.ds(0, channels)], one["vr"])
+    drain(ps_v.at[pl.ds(0, 2 * (channels - part_rows))], one["vr"])
     total = dot(state_out, ps_v[:2 * channels])
     drain(pi_ref, one["pr"])
+    drain(pd_ref, one["qr"])
     base = acc_ref[...] + pi_ref[0].astype(F32) + pi_ref[1].astype(F32)
     total = total + jnp.concatenate(
-        [base[inner_rows:inner_rows + edge], base[:inner_rows], base[inner_rows + edge:]], axis=0)
+        [base[inner_rows:inner_rows + edge], base[:direct_rows] + pd_ref[...].astype(F32),
+         base[direct_rows:inner_rows], base[inner_rows + edge:]], axis=0)
     state_copy.wait_recv()
     out_ref[...] = (total + dot(so_in[...], ps_v[2 * channels:])).astype(BF16)
 
     pl.when(not_last)(halo_up.wait_send)
     pl.when(not_first)(halo_down.wait_send)
+    forwarded = w_all.at[pl.ds(0, (2 * last + 1) * cw * half_rows // (4 * channels)), :]
     for ref, name in (
-            (x_ref, "as"), (x_ref, "fs"), (others, "gs"), (el_all.at[far], "is"),
-            (e_all.at[:, far], "es"), (po_ref, "ps"), (ps_v.at[pl.ds(0, 2 * channels)], "ws"),
-            (ps_v.at[pl.ds(0, channels)], "vs"), (par_ref.at[0], "os"), (cq_ref.at[0], "cs"),
+            (x_ref, "as"), (x_ref, "bs"), (forwarded, "fs"), (gains, "gs"), (x_full.at[0, 0, lower], "ds"), (el_all.at[far], "is"),
+            (e_all.at[:, far], "es"), (po_ref, "ps"), (ps_v.at[pl.ds(0, channels + 2 * part_rows)], "ws"),
+            (ps_v.at[pl.ds(0, 2 * (channels - part_rows))], "vs"), (par_ref.at[0], "os"), (cq_ref.at[0], "cs"),
             (rp_out, "rs"), (so_ref, "ss")):
         drain(ref, one[name])
 
@@ -627,7 +690,7 @@
             pltpu.VMEM((2, dirs * groups * group, per), F32),
             pltpu.VMEM((2, dirs * groups * group, per), F32),
             pltpu.VMEM((n_tp, CHUNKS, rows, cw), BF16),
-            pltpu.VMEM((n_tp, 1, width), F32),
+            pltpu.VMEM((n_tp - 1, 1, width), F32),
             pltpu.VMEM((n_sp, 1, rows), F32),
             packed, packed, packed, packed, packed, packed, packed, packed, packed, packed,
             pltpu.VMEM((2, rows, states), F32),
@@ -647,13 +710,14 @@
             pltpu.VMEM((3, rows, width), BF16),
             pltpu.VMEM((rows, width), BF16),
             pltpu.VMEM((2, rows, width), BF16),
+            pltpu.VMEM((32, width), BF16),
             pltpu.VMEM((rows, width), F32),
             pltpu.VMEM((rows, 2 * channels), BF16),
             pltpu.VMEM((rows, 2 * channels), BF16),
             pltpu.VMEM((rows, channels), BF16),
             pltpu.VMEM((rows, channels), BF16),
-            pltpu.VMEM((rows - 32, width), F32),
-            dma(12), dma(CHUNKS), dma(CHUNKS), dma(24), dma(2), dma(2), dma(2),
+            pltpu.VMEM((rows, width), BF16),
+            dma(12), dma(CHUNKS), dma(CHUNKS + 1), dma(n_tp - 1), dma(26), dma(2), dma(2), dma(2),
             pltpu.SemaphoreType.REGULAR((max(2, (n_sp - 1).bit_length()),)),
             pltpu.SemaphoreType.REGULAR,
         ],

time: 19.1 us -> 18.7 us (0.979)
  Pallas kernels: 18.3 us -> 17.9 us
    pallas_call x1, Pallas kernels: 18.3 us -> 17.9 us  [per_device(): pl.pallas_call(functools.partial(kernel, n_sp, n_tp), out_shape=jax.Shape...]
where the time goes in v4:
time: 18.7 us; the launch traced here: 18.6 us
  Pallas kernels  17.9 us (96%)
  local copies, waits for them, and re-layouts  0.66 us (4%)
    pallas_call x1, Pallas kernels, per_device(): pl.pallas_call(functools.partial(kernel, n_sp, n_tp), out_shape=jax.Shape...  17.9 us
    unnamed x1, local copies, waits for them, and re-layouts  0.66 us

profile of v4, /device:TPU:0, one launch (start us, length us, event | category | flops | bytes accessed | tf_op | source)
XLA Modules:
  0.0 18.6 jit_solution(15464103976726022085)
XLA Ops:
  0.0 17.9 %shard_map.172 = bf16[128,512]{1,0:T(8,128)(2,1)S(1)} custom-call(bf16[128,512]{1,0:T(8,128)(2,1)} %x_hbm.1, f32[1,512]{1,0:T(1,128)} %bitcast.21, bf16[2048,128]{1,0:T(8,128)(2,1)} %wv.1, bf16[2048,128]{1,0:T(8,128)(2,1)} %wm.1, bf16[2048,128]{1,0:T(8,128)(2,1)} %wg.1, bf16[2048,128]{1,0:T(8,128)(2,1)} %ws.1, f32[3,128]{1,0:T(4,128)} %taps_hbm.1, ...), custom_call_target="tpu_custom_call" | custom-call | tf_op jit(solution)/shard_map/pallas_call | solution.py:674
  17.9 0.7 %copy.20 = bf16[128,512]{1,0:T(8,128)(2,1)} copy(bf16[128,512]{1,0:T(8,128)(2,1)S(1)} %shard_map.172) | data formatting | bytes 262144

commit v5 on v4

--- a/solution.py
+++ b/solution.py
@@ -74,7 +74,7 @@
     out_ref,
     x_ref, gain_ref, taps_ref, skip_ref, par_ref, iv_s, iv_v,
     w_all, pc_v, ps_v, in_v, rd_v, x_full, gains, el_all, fr_ref, fi_ref, gr_ref, gi_ref,
-    dr_ref, di_ref, hr_ref, hi_ref, kr_ref, ki_ref, k_row, d_row, p_row,
+    dr_ref, di_ref, hr_ref, hi_ref, kr_ref, ki_ref, k_row, p_row,
     bt_ref, rt_ref, rc_ref, cq_ref, src_ref, halo_ref, e_out, e_all,
     span_ref, wa_ref, wb_ref, po_ref, p1_in, pi_ref, pd_ref, acc_ref, so_ref, so_in,
     rp_out, rp_in, xs_ref,
@@ -89,8 +89,7 @@
     diag = (1 - y) * 2 + 1 - core
     cw = width // CHUNKS
 
-    names = ("bs", "as", "ar", "fs", "gs", "ds", "dr", "is", "ir", "es", "er", "ps", "pr", "ws", "wr",
-             "vs", "vr", "qr", "os", "or", "cs", "cr", "rs", "rr", "ss", "sr")
+    names = ("out", "gs", "os", "is", "es", "ar", "dr", "fr", "ir", "er", "pr", "wr", "vr", "or", "rr", "sr")
     one = {name: one_sem.at[i] for i, name in enumerate(names)}
     loads = {}
 
@@ -107,6 +106,9 @@
 
     def drain(ref, sem):
         remote(ref, ref, sem, sem, {"tp": sib}).wait_recv()
+
+    def drain_rows(count, sem):
+        drain(w_all.at[pl.ds(0, count)], sem)
 
     def loaded(*names):
         for name in names:
@@ -169,15 +171,15 @@
 
     spans = [(c, None) for c in range(last)] + [(last, upper), (last, lower)]
     to_oth = [
-        remote(block(x_ref, *span), landing(tp, *span), one["bs"], br_sem.at[i], {"tp": oth})
+        remote(block(x_ref, *span), landing(tp, *span), one["out"], br_sem.at[i], {"tp": oth})
         for i, span in enumerate(spans)
     ]
-    to_sib = remote(x_ref, xs_ref, one["as"], one["ar"], {"tp": sib})
+    to_sib = remote(x_ref, xs_ref, one["out"], one["ar"], {"tp": sib})
     forward = [
-        remote(landing(oth, *span), landing(oth, *span), one["fs"], fwr_sem.at[i], {"tp": sib})
+        remote(landing(oth, *span), landing(oth, *span), one["out"], one["fr"] if i < last else fwr_sem, {"tp": sib})
         for i, span in enumerate(spans[:-1])
     ]
-    to_diag = remote(block(x_ref, *spans[-1]), landing(tp, *spans[-1]), one["ds"], one["dr"],
+    to_diag = remote(block(x_ref, *spans[-1]), landing(tp, *spans[-1]), one["out"], one["dr"],
                      {"tp": diag})
     gain_copies = [
         remote(gain_ref, gains.at[j], one["gs"], gr_sem.at[j], {"tp": peer})
@@ -201,7 +203,7 @@
         return ps_v.at[pl.ds(pos * channels + my_part, part_rows)]
 
     weight_copies = [
-        remote(src, dst, one["ws"], one["wr"], {"tp": peer})
+        remote(src, dst, one["out"], one["wr"], {"tp": peer})
         for src, dst, peer in (
             (ps.at[pl.ds(my_part, part_rows), columns(oth)], slot(1), oth),
             (ps.at[pl.ds(my_part, part_rows), columns(diag)], slot(3), diag),
@@ -209,14 +211,14 @@
         )
     ]
     weight_forward = [
-        remote(slot(pos), slot(pos), one["vs"], one["vr"], {"sp": mate})
+        remote(slot(pos), slot(pos), one["out"], one["vr"], {"sp": mate})
         for mate in mates for pos in (1, 3)
     ]
     other_copies = [
         remote(src, par_ref.at[1, at], one["os"], one["or"], {"tp": oth})
         for src, at in zip(par_hbm, par_parts)
-    ] + [remote(cq_ref.at[0], cq_ref.at[1], one["cs"], one["cr"], {"tp": oth})]
-    rest_copy = remote(rp_out, rp_in, one["rs"], one["rr"], {"tp": oth})
+    ] + [remote(cq_ref.at[0], cq_ref.at[1], one["out"], one["rr"], {"tp": oth})]
+    rest_copy = remote(rp_out, rp_in, one["out"], one["rr"], {"tp": oth})
 
     def pass_on(c):
         to_oth[c].wait_recv()
@@ -362,8 +364,7 @@
     loaded("ivv")
     repeat(1, n_sp, lambda r: interval_copy(r).start())
     gain_copies[2].wait_recv()
-    for c in range(last):
-        forward[c].wait_recv()
+    drain(x_full.at[0, pl.ds(0, last)], one["fr"])
     t, s = project(chunks_of(diag, last), gains[2][:, :last * cw], diag, last * cw)
     projected, squares = projected + t, squares + s
     to_oth[last + 1].wait_recv()
@@ -402,8 +403,10 @@
             lanes = slice(d * half + i * 256, d * half + (i + 1) * 256)
             dr = dot(state_input, bt_ref[0, :, lanes])
             di = dot(state_input, bt_ref[1, :, lanes])
-            d_row[0, :, lanes] = dr
-            d_row[1, :, lanes] = di
+            for h in range(2):
+                tile = pl.ds(d * 4 + i * 2 + h, rows, stride=8)
+                dr_ref[tile, :] = dr[:, h * 128:(h + 1) * 128]
+                di_ref[tile, :] = di[:, h * 128:(h + 1) * 128]
             kr, ki = k_row[0, :, lanes], k_row[1, :, lanes]
             er = jnp.sum(kr * dr - ki * di, axis=0, keepdims=True)
             ei = jnp.sum(kr * di + ki * dr, axis=0, keepdims=True)
@@ -447,7 +450,7 @@
     def offer(branch, i, span):
         at = pl.ds(*span)
         po_ref[0, at, :] = dot(branch, pc_v[:, columns(diag)]).astype(BF16)
-        copy = remote(po_ref.at[0, at], p1_in.at[at], one["ps"], p1r_sem.at[i], {"tp": sib})
+        copy = remote(po_ref.at[0, at], p1_in.at[at], one["out"], p1r_sem.at[i], {"tp": sib})
         copy.start()
         return copy
 
@@ -455,20 +458,20 @@
         at = pl.ds(*span)
         kept = dot(branch, pc_v[:, columns(oth)])
         po_ref[2, at, :] = (kept + p1_in[at, :].astype(F32)).astype(BF16)
-        copy = remote(po_ref.at[2, at], pi_ref.at[1, at], one["ps"], one["pr"], {"tp": oth})
+        copy = remote(po_ref.at[2, at], pi_ref.at[1, at], one["out"], one["pr"], {"tp": oth})
         copy.start()
 
     def rest_of(branch, span):
         at = pl.ds(*span)
         po_ref[1, at, :] = dot(branch, pc_v[:, columns(sib)]).astype(BF16)
-        copy = remote(po_ref.at[1, at], pi_ref.at[0, at], one["ps"], one["pr"], {"tp": sib})
+        copy = remote(po_ref.at[1, at], pi_ref.at[0, at], one["out"], one["pr"], {"tp": sib})
         copy.start()
         acc_ref[at, :] = dot(branch, pc_v[:, columns(tp)])
 
     direct = pl.ds(0, direct_rows)
     direct_copies = [
-        remote(po_ref.at[2, direct], pi_ref.at[1, direct], one["ps"], one["pr"], {"tp": oth}),
-        remote(po_ref.at[0, direct], pd_ref, one["ps"], one["qr"], {"tp": diag}),
+        remote(po_ref.at[2, direct], pi_ref.at[1, direct], one["out"], one["pr"], {"tp": oth}),
+        remote(po_ref.at[0, direct], pd_ref, one["out"], one["pr"], {"tp": diag}),
     ]
     for copy, at, owner in zip(direct_copies, (2, 0), (oth, diag)):
         po_ref[at, direct, :] = dot(conv_out[:direct_rows], pc_v[:, columns(owner)]).astype(BF16)
@@ -476,10 +479,6 @@
     offered = offer(conv_out[direct_rows:], 0, middle)
 
     find_edges(0)
-
-    for part, ref in ((0, dr_ref), (1, di_ref)):
-        for j in range(8):
-            ref[pl.ds(j, rows, stride=8), :] = d_row[part, :, j * 128:(j + 1) * 128]
 
     send_edges(1, n_sp - sp)
     drain(ps_v.at[pl.ds(0, channels + 2 * part_rows)], one["wr"])
@@ -604,8 +603,7 @@
         for s in range(2)
     ]
 
-    rest_copy.wait_recv()
-    drain(cq_ref.at[1], one["cr"])
+    drain_rows((rows * channels + cq_ref.size // 2) // width, one["rr"])
     drain(e_all.at[:, far], one["er"])
     for s in range(2):
         def combine(r, carry):
@@ -633,12 +631,11 @@
         gated.append((0.5 * full * (1.0 + jnp.tanh(inner))).astype(BF16))
     state_out = jnp.concatenate(gated, axis=1)
     so_ref[...] = state_out
-    state_copy = remote(so_ref, so_in, one["ss"], one["sr"], {"tp": sib})
+    state_copy = remote(so_ref, so_in, one["out"], one["sr"], {"tp": sib})
     state_copy.start()
     drain(ps_v.at[pl.ds(0, 2 * (channels - part_rows))], one["vr"])
     total = dot(state_out, ps_v[:2 * channels])
-    drain(pi_ref, one["pr"])
-    drain(pd_ref, one["qr"])
+    drain_rows(2 * rows + direct_rows, one["pr"])
     base = acc_ref[...] + pi_ref[0].astype(F32) + pi_ref[1].astype(F32)
     total = total + jnp.concatenate(
         [base[inner_rows:inner_rows + edge], base[:direct_rows] + pd_ref[...].astype(F32),
@@ -648,13 +645,16 @@
 
     pl.when(not_last)(halo_up.wait_send)
     pl.when(not_first)(halo_down.wait_send)
-    forwarded = w_all.at[pl.ds(0, (2 * last + 1) * cw * half_rows // (4 * channels)), :]
-    for ref, name in (
-            (x_ref, "as"), (x_ref, "bs"), (forwarded, "fs"), (gains, "gs"), (x_full.at[0, 0, lower], "ds"), (el_all.at[far], "is"),
-            (e_all.at[:, far], "es"), (po_ref, "ps"), (ps_v.at[pl.ds(0, channels + 2 * part_rows)], "ws"),
-            (ps_v.at[pl.ds(0, 2 * (channels - part_rows))], "vs"), (par_ref.at[0], "os"), (cq_ref.at[0], "cs"),
-            (rp_out, "rs"), (so_ref, "ss")):
-        drain(ref, one[name])
+    sent = [(x_ref, 2), (x_full.at[0, pl.ds(0, last)], 1), (x_full.at[0, 0], 1), (po_ref, 1),
+            (ps_v.at[pl.ds(0, channels + 2 * part_rows)], 1),
+            (ps_v.at[pl.ds(0, 2 * (channels - part_rows))], 1), (cq_ref.at[0], 1), (rp_out, 1),
+            (so_ref, 1)]
+    count = sum(times * ref.size for ref, times in sent) // width
+    drain_rows(count, one["out"])
+    drain(par_ref.at[0], one["os"])
+    drain(gains, one["gs"])
+    drain(el_all.at[far], one["is"])
+    drain(e_all.at[:, far], one["es"])
 
 
 def per_device(
@@ -694,7 +694,6 @@
             pltpu.VMEM((n_sp, 1, rows), F32),
             packed, packed, packed, packed, packed, packed, packed, packed, packed, packed,
             pltpu.VMEM((2, rows, states), F32),
-            pltpu.VMEM((2, rows, states), F32),
             pltpu.VMEM((2, rows, 2 * states), BF16),
             pltpu.VMEM((2, channels, states), BF16),
             pltpu.VMEM((2, channels, states), BF16),
@@ -717,7 +716,7 @@
             pltpu.VMEM((rows, channels), BF16),
             pltpu.VMEM((rows, channels), BF16),
             pltpu.VMEM((rows, width), BF16),
-            dma(12), dma(CHUNKS), dma(CHUNKS + 1), dma(n_tp - 1), dma(26), dma(2), dma(2), dma(2),
+            dma(12), pltpu.SemaphoreType.DMA, dma(CHUNKS + 1), dma(n_tp - 1), dma(16), dma(2), dma(2), dma(2),
             pltpu.SemaphoreType.REGULAR((max(2, (n_sp - 1).bit_length()),)),
             pltpu.SemaphoreType.REGULAR,
         ],

time: 18.7 us -> 18.5 us (0.989)
  Pallas kernels: 17.9 us -> 17.7 us
    pallas_call x1, Pallas kernels: 17.9 us -> 17.7 us  [per_device(): pl.pallas_call(functools.partial(kernel, n_sp, n_tp), out_shape=jax.Shape...]
where the time goes in v5:
time: 18.5 us; the launch traced here: 18.4 us
  Pallas kernels  17.7 us (96%)
  local copies, waits for them, and re-layouts  0.66 us (4%)
    pallas_call x1, Pallas kernels, per_device(): pl.pallas_call(functools.partial(kernel, n_sp, n_tp), out_shape=jax.Shape...  17.7 us
    unnamed x1, local copies, waits for them, and re-layouts  0.66 us

profile of v5, /device:TPU:0, one launch (start us, length us, event | category | flops | bytes accessed | tf_op | source)
XLA Modules:
  0.0 18.4 jit_solution(6228714290541802854)
XLA Ops:
  0.0 17.7 %shard_map.172 = bf16[128,512]{1,0:T(8,128)(2,1)S(1)} custom-call(bf16[128,512]{1,0:T(8,128)(2,1)} %x_hbm.1, f32[1,512]{1,0:T(1,128)} %bitcast.21, bf16[2048,128]{1,0:T(8,128)(2,1)} %wv.1, bf16[2048,128]{1,0:T(8,128)(2,1)} %wm.1, bf16[2048,128]{1,0:T(8,128)(2,1)} %wg.1, bf16[2048,128]{1,0:T(8,128)(2,1)} %ws.1, f32[3,128]{1,0:T(4,128)} %taps_hbm.1, ...), custom_call_target="tpu_custom_call" | custom-call | tf_op jit(solution)/shard_map/pallas_call | solution.py:674
  17.7 0.7 %copy.20 = bf16[128,512]{1,0:T(8,128)(2,1)} copy(bf16[128,512]{1,0:T(8,128)(2,1)S(1)} %shard_map.172) | data formatting | bytes 262144

commit v6 on v5

--- a/solution.py
+++ b/solution.py
@@ -75,7 +75,7 @@
     x_ref, gain_ref, taps_ref, skip_ref, par_ref, iv_s, iv_v,
     w_all, pc_v, ps_v, in_v, rd_v, x_full, gains, el_all, fr_ref, fi_ref, gr_ref, gi_ref,
     dr_ref, di_ref, hr_ref, hi_ref, kr_ref, ki_ref, k_row, p_row,
-    bt_ref, rt_ref, rc_ref, cq_ref, src_ref, halo_ref, e_out, e_all,
+    bt_ref, rt_ref, rc_ref, cq_ref, src_ref, halo_ref, e_f32, e_out, e_all,
     span_ref, wa_ref, wb_ref, po_ref, p1_in, pi_ref, pd_ref, acc_ref, so_ref, so_in,
     rp_out, rp_in, xs_ref,
     load_sem, fwr_sem, br_sem, gr_sem, one_sem, hs_sem, hr_sem, p1r_sem, greet_sem, pair_sem,
@@ -131,12 +131,12 @@
         pl.semaphore_wait(greet_sem.at[k], near_count(1 << k))
 
     rounds = greet_sem.shape[0]
+    load("x", x_ref, (x_hbm, x_ref))
     barrier = pltpu.get_barrier_semaphore()
     for peer in (sib, oth):
         pl.semaphore_signal(barrier, inc=1, device_id={"tp": peer}, device_id_type=MESH)
     near(1, lambda where: pl.semaphore_signal(
         barrier, inc=1, device_id={"sp": where}, device_id_type=MESH))
-    load("x", x_ref, (x_hbm, x_ref))
     iv_load = pltpu.make_async_copy(iv_hbm, iv_s, load_sem.at[len(loads)])
     iv_load.start()
     loads["iv"] = None
@@ -412,8 +412,9 @@
             ei = jnp.sum(kr * di + ki * dr, axis=0, keepdims=True)
             for h in range(2):
                 q = i * 2 + h
-                e_out[d, q:q + 1, :] = er[:, h * 128:(h + 1) * 128]
-                e_out[d, 4 + q:5 + q, :] = ei[:, h * 128:(h + 1) * 128]
+                e_f32[d, q:q + 1, :] = er[:, h * 128:(h + 1) * 128]
+                e_f32[d, 4 + q:5 + q, :] = ei[:, h * 128:(h + 1) * 128]
+        e_out[d] = e_f32[d].astype(BF16)
 
     find_edges(1)
     send_edges(n_sp - sp, n_sp)
@@ -608,7 +609,7 @@
     for s in range(2):
         def combine(r, carry):
             h0, h1 = carry
-            moved = apply((wa_ref[s, r], wb_ref[s, r]), e_all[s, r])
+            moved = apply((wa_ref[s, r], wb_ref[s, r]), e_all[s, r].astype(F32))
             mine = sp - r >= 0
             return h0 + jnp.where(mine, moved, 0.0), h1 + jnp.where(mine, 0.0, moved)
 
@@ -702,7 +703,8 @@
             pltpu.VMEM((rows, channels), BF16),
             pltpu.VMEM((2, 16, channels), BF16),
             pltpu.VMEM((2, 8, 128), F32),
-            pltpu.VMEM((2, n_sp, 8, 128), F32),
+            pltpu.VMEM((2, 8, 128), BF16),
+            pltpu.VMEM((2, n_sp, 8, 128), BF16),
             pltpu.VMEM((n_sp, 1, 128), F32),
             pltpu.VMEM((2, n_sp, 8, 128), F32),
             pltpu.VMEM((2, n_sp, 8, 128), F32),

time: 18.5 us -> 18.4 us (level)
  no operation moved by 1% of the time
where the time goes in v6:
time: 18.4 us; the launch traced here: 18.3 us
  Pallas kernels  17.6 us (96%)
  local copies, waits for them, and re-layouts  0.66 us (4%)
    pallas_call x1, Pallas kernels, per_device(): pl.pallas_call(functools.partial(kernel, n_sp, n_tp), out_shape=jax.Shape...  17.6 us
    unnamed x1, local copies, waits for them, and re-layouts  0.66 us

profile of v6, /device:TPU:0, one launch (start us, length us, event | category | flops | bytes accessed | tf_op | source)
XLA Modules:
  0.0 18.3 jit_solution(4891998944782066410)
XLA Ops:
  0.0 17.6 %shard_map.172 = bf16[128,512]{1,0:T(8,128)(2,1)S(1)} custom-call(bf16[128,512]{1,0:T(8,128)(2,1)} %x_hbm.1, f32[1,512]{1,0:T(1,128)} %bitcast.21, bf16[2048,128]{1,0:T(8,128)(2,1)} %wv.1, bf16[2048,128]{1,0:T(8,128)(2,1)} %wm.1, bf16[2048,128]{1,0:T(8,128)(2,1)} %wg.1, bf16[2048,128]{1,0:T(8,128)(2,1)} %ws.1, f32[3,128]{1,0:T(4,128)} %taps_hbm.1, ...), custom_call_target="tpu_custom_call" | custom-call | tf_op jit(solution)/shard_map/pallas_call | solution.py:675
  17.6 0.7 %copy.20 = bf16[128,512]{1,0:T(8,128)(2,1)} copy(bf16[128,512]{1,0:T(8,128)(2,1)S(1)} %shard_map.172) | data formatting | bytes 262144
